TPU v7x, 256 devices: a whole 4x4x8 slice. The times are simulated.
256 devices in a mesh: sp: 64 (over z, x, core), tp: 4 (over y).
Axes of the slice: x: 4, y: 4, z: 8, core: 2. Of those that a mesh axis runs over, the one named last changes fastest.
Arguments:
- tokens: bfloat16 [16384, 1024], P(('sp', 'tp')), may hold values from -6 to 6
- norm_gain: float32 [1024], replicated, may hold values from 0.1 to 1.9
- w_query: bfloat16 [1024, 1024], P('sp', 'tp'), may hold values from -0.1875 to 0.1875
- w_key: bfloat16 [1024, 1024], P('sp', 'tp'), may hold values from -0.1875 to 0.1875
- w_value: bfloat16 [1024, 1024], P('sp', 'tp'), may hold values from -0.1875 to 0.1875
- w_forget: bfloat16 [1024, 16], P('sp', 'tp'), may hold values from -0.375 to 0.375
- forget_offset: float32 [16], P('tp'), may hold values from 1 to 3.5
- w_out_t: bfloat16 [1024, 1024], P('sp', 'tp'), may hold values from -0.1875 to 0.1875
- out_gain: float32 [1024], replicated, may hold values from 0.1 to 1.9
Outputs:
- mixed: bfloat16 [16384, 1024], P(('sp', 'tp'))
All inputs are finite; a program needn't handle non-finite values.
Results may differ from a plain program's by a relative error of at most 0.015.
Values may be sent and summed in bfloat16 or wider, within the bound.
A program may use at most 192 MiB of HBM per device.

v0:
```python
import jax
import jax.numpy as jnp
from jax import lax
from jax.sharding import Mesh
from jax.sharding import PartitionSpec as P

HEAD_DIM = 64
SP = ("sp_0", "sp_1", "sp_2")
SP_TP = ("sp_0", "sp_1", "sp_2", "tp")


norm_eps = 1e-06
masked_score = -1e30


def joined_along(parts, dim):
    shape = list(parts.shape[1:])
    shape[dim] *= parts.shape[0]
    return jnp.moveaxis(parts, 0, dim).reshape(shape)


def gather_in_order(shard, axes, turns):
    parts = shard
    for k in turns:
        parts = lax.all_gather(parts, axes[k])
    done = turns[::-1]
    back = [done.index(k) for k in range(len(axes))]
    parts = parts.transpose(*back, *range(len(axes), parts.ndim))
    return parts.reshape(-1, *shard.shape)


def gathered_by_axis(shard, axes, turns, dim):
    return joined_along(gather_in_order(shard, axes, turns), dim)


def over_axes(shard, axes, turns, dim, absorb, carry):
    everything = jax.tree.map(lambda part: gathered_by_axis(part, axes, turns, dim), shard)
    return absorb(carry, everything, jnp.int32(0))


def over_all(section, axis, dim, turn, start):
    def gathered(part):
        return lax.all_gather(part, axis, axis=dim, tiled=True)

    return turn(start, jax.tree.map(gathered, section), jnp.int32(0))


def own_rows(portion, width, axis):
    count = width * lax.axis_size(axis)
    sent = portion(jnp.int32(0), count).astype(jnp.bfloat16)
    return lax.psum_scatter(sent, axis, scatter_dimension=0, tiled=True).astype(jnp.float32)


def rms_norm(values_in, gain_row):
    floats = values_in.astype(jnp.float32)
    scale_row = lax.rsqrt(jnp.mean(floats * floats, axis=-1, keepdims=True) + norm_eps)
    return (floats * scale_row * gain_row).astype(jnp.bfloat16)


def shards(tokens, norm_gain, w_query, w_key, w_value, w_forget, forget_offset, w_out_t, out_gain):
    normed = rms_norm(tokens, norm_gain)
    width_local = w_query.shape[1]
    heads_local = w_forget.shape[1]
    tok_block = normed.shape[0] * lax.axis_size("tp")
    total_tokens = tok_block * lax.axis_size(SP)
    all_rows = lax.all_gather(normed, "tp", axis=0, tiled=True)

    def add_piece(state_now, pieces, first_row):
        columns = lax.dynamic_slice_in_dim(all_rows, first_row, pieces[0].shape[0], 1)
        joined_piece = jnp.concatenate(pieces, axis=1)
        return state_now + jnp.dot(columns, joined_piece, preferred_element_type=jnp.float32)

    empty = jnp.zeros((tok_block, 3 * width_local + heads_local), jnp.float32)
    projected_cols = over_axes(
        (w_query, w_key, w_value, w_forget), SP, (1, 0, 2), 0, add_piece, empty
    )
    out_weight = lax.all_gather(w_out_t, SP, axis=0, tiled=True)
    head_shape = (tok_block, heads_local, HEAD_DIM)
    queries = projected_cols[:, :width_local].astype(jnp.bfloat16).reshape(head_shape)
    keys_here = (
        projected_cols[:, width_local : 2 * width_local].astype(jnp.bfloat16).reshape(head_shape)
    )
    values_here = (
        projected_cols[:, 2 * width_local : 3 * width_local]
        .astype(jnp.bfloat16)
        .reshape(head_shape)
    )
    logits = (
        projected_cols[:, 3 * width_local :] + forget_offset + jnp.log(jnp.float32(total_tokens))
    )
    log_gates = jax.nn.log_sigmoid(logits)
    all_gates = gathered_by_axis(log_gates, (("sp_0", "sp_1"), "sp_2"), (0, 1), 0)
    cumulative = jnp.cumsum(all_gates, axis=0)
    offset = lax.axis_index(SP) * tok_block
    cum_query = lax.dynamic_slice_in_dim(cumulative, offset, tok_block, 0)
    query_pos = offset + jnp.arange(tok_block, dtype=jnp.int32)
    score_scale = HEAD_DIM ** (-0.5)

    def absorb(state_now, pieces, first_row):
        run_max, run_sum, run_acc = state_now
        key_piece, value_piece = pieces
        span_len = key_piece.shape[0]
        cum_key = lax.dynamic_slice_in_dim(cumulative, first_row, span_len, 0)
        scores = (
            jnp.einsum("qhd,khd->hqk", queries, key_piece, preferred_element_type=jnp.float32)
            * score_scale
        )
        scores = scores + cum_query.T[:, :, None] - cum_key.T[:, None, :]
        key_pos = first_row + jnp.arange(span_len, dtype=jnp.int32)
        allowed = (key_pos[None, :] <= query_pos[:, None])[None]
        scores = jnp.where(allowed, scores, masked_score)
        new_max = jnp.maximum(run_max, jnp.max(scores, axis=-1))
        shares = jnp.where(allowed, jnp.exp(scores - new_max[..., None]), 0.0)
        rescale = jnp.exp(run_max - new_max)
        new_sum = run_sum * rescale + jnp.sum(shares, axis=-1)
        new_acc = run_acc * rescale[..., None] + jnp.einsum(
            "hqk,khd->hqd", shares, value_piece.astype(jnp.float32), precision=lax.Precision.DEFAULT
        )
        return (new_max, new_sum, new_acc)

    start_state = (
        jnp.full((heads_local, tok_block), masked_score, jnp.float32),
        jnp.zeros((heads_local, tok_block), jnp.float32),
        jnp.zeros((heads_local, tok_block, HEAD_DIM), jnp.float32),
    )
    run_max, run_sum, run_acc = over_all((keys_here, values_here), SP, 0, absorb, start_state)
    attended = (
        (run_acc / run_sum[..., None])
        .transpose(1, 0, 2)
        .reshape(tok_block, width_local)
        .astype(jnp.bfloat16)
    )
    rows_mine = tokens.shape[0]

    def out_term(first_row, row_count):
        block_rows = lax.dynamic_slice_in_dim(attended, first_row, row_count, 0)
        return lax.dot_general(
            block_rows, out_weight, (((1,), (1,)), ((), ())), preferred_element_type=jnp.float32
        )

    projected = own_rows(out_term, rows_mine, "tp")
    return rms_norm(projected, out_gain)


def solution(mesh):
    finer = Mesh(mesh.devices.reshape(8, 4, 2, mesh.shape["tp"]), ("sp_0", "sp_1", "sp_2", "tp"))
    return jax.shard_map(
        shards,
        mesh=finer,
        in_specs=(
            P(SP_TP, None),
            P(),
            P(SP, "tp"),
            P(SP, "tp"),
            P(SP, "tp"),
            P(SP, "tp"),
            P("tp"),
            P(SP, "tp"),
            P(),
        ),
        out_specs=P(SP_TP, None),
        check_vma=False,
    )
```

profile of v0, /device:TPU:224, one launch (start us, length us, event | category | flops | bytes accessed | tf_op | source)
XLA Modules:
  0.0 413.9 jit_solution(9848764265718067449)
XLA Ops:
  6.5 0.0 all-gather.18.cloned.1.call-start
  6.5 12.4 %all-gather.6 = bf16[64,256]{1,0:T(8,128)(2,1)S(1)} all-gather(bf16[16,256]{1,0:T(8,128)(2,1)} %param.13), channel_id=8, replica_groups=mesh['sp_0'=8,'sp_1'=4,'sp_2'=2,'tp'=4] {'sp_1'}, dimensions={0}, use_global_device_ids=true | all-gather | bytes 40960 | tf_op jit(solution)/shard_map/all_gather | solution.py:25
  18.9 24.8 %all-gather.7 = bf16[32,16,256]{2,1,0:T(8,128)(2,1)S(1)} all-gather(bf16[4,16,256]{2,1,0:T(8,128)(2,1)S(1)} %bitcast.95), channel_id=9, replica_groups=mesh['sp_0'=8,'sp_1'=4,'sp_2'=2,'tp'=4] {'sp_0'}, dimensions={0}, use_global_device_ids=true | all-gather | bytes 294912 | tf_op jit(solution)/shard_map/all_gather | solution.py:25
  43.7 2.2 all-gather.8
  45.9 0.1 copy.32
  45.9 12.0 %all-gather = bf16[64,256]{1,0:T(8,128)(2,1)S(1)} all-gather(bf16[16,256]{1,0:T(8,128)(2,1)} %param.11), channel_id=2, replica_groups=mesh['sp_0'=8,'sp_1'=4,'sp_2'=2,'tp'=4] {'sp_1'}, dimensions={0}, use_global_device_ids=true | all-gather | bytes 40960 | tf_op jit(solution)/shard_map/all_gather | solution.py:25
  57.9 24.9 %all-gather.1 = bf16[32,16,256]{2,1,0:T(8,128)(2,1)S(1)} all-gather(bf16[4,16,256]{2,1,0:T(8,128)(2,1)S(1)} %bitcast.96), channel_id=3, replica_groups=mesh['sp_0'=8,'sp_1'=4,'sp_2'=2,'tp'=4] {'sp_0'}, dimensions={0}, use_global_device_ids=true | all-gather | bytes 294912 | tf_op jit(solution)/shard_map/all_gather | solution.py:25
  82.8 2.2 all-gather.2
  85.0 0.1 copy.30
  85.1 12.0 %all-gather.3 = bf16[64,256]{1,0:T(8,128)(2,1)S(1)} all-gather(bf16[16,256]{1,0:T(8,128)(2,1)} %param.12), channel_id=5, replica_groups=mesh['sp_0'=8,'sp_1'=4,'sp_2'=2,'tp'=4] {'sp_1'}, dimensions={0}, use_global_device_ids=true | all-gather | bytes 40960 | tf_op jit(solution)/shard_map/all_gather | solution.py:25
  97.1 24.9 %all-gather.4 = bf16[32,16,256]{2,1,0:T(8,128)(2,1)S(1)} all-gather(bf16[4,16,256]{2,1,0:T(8,128)(2,1)S(1)} %bitcast.97), channel_id=6, replica_groups=mesh['sp_0'=8,'sp_1'=4,'sp_2'=2,'tp'=4] {'sp_0'}, dimensions={0}, use_global_device_ids=true | all-gather | bytes 294912 | tf_op jit(solution)/shard_map/all_gather | solution.py:25
  122.0 2.2 all-gather.5
  124.2 0.1 copy.31
  124.2 1.0 fusion.22
  125.3 1.0 fusion.24
  126.3 13.3 %all_gather.96 = bf16[256,1024]{1,0:T(8,128)(2,1)S(1)} all-gather(bf16[64,1024]{1,0:T(8,128)(2,1)S(1)} %fusion.24), channel_id=1, replica_groups=mesh['sp_0'=8,'sp_1'=4,'sp_2'=2,'tp'=4] {'tp'}, dimensions={0}, use_global_device_ids=true | all-gather | bytes 655360 | tf_op jit(solution)/shard_map/all_gather | solution.py:66
  139.6 9.6 %all-gather.14 = bf16[4,16,4]{1,2,0:T(4,128)(2,1)S(1)} all-gather(bf16[1,16,4]{1,2,0:T(4,128)(2,1)} %bitcast.101), channel_id=11, replica_groups=mesh['sp_0'=8,'sp_1'=4,'sp_2'=2,'tp'=4] {'sp_1'}, dimensions={0}, use_global_device_ids=true | all-gather | bytes 640 | tf_op jit(solution)/shard_map/all_gather | solution.py:25
  149.2 24.5 %all-gather.10 = bf16[32,16,4]{1,2,0:T(4,128)(2,1)S(1)} all-gather(bf16[4,16,4]{1,2,0:T(4,128)(2,1)S(1)} %all-gather.14), channel_id=12, replica_groups=mesh['sp_0'=8,'sp_1'=4,'sp_2'=2,'tp'=4] {'sp_0'}, dimensions={0}, use_global_device_ids=true | all-gather | bytes 4608 | tf_op jit(solution)/shard_map/all_gather | solution.py:25
  173.7 1.9 all-gather.11
  175.5 0.5 copy.40
  176.0 0.8 fusion.36
  176.8 0.7 fusion.35
  177.5 0.0 all-gather.18.cloned.1.call-update
  177.6 0.0 all-gather.20.cloned.1.call-start
  177.6 0.7 all-gather.20.cloned.1.call-update
  178.3 0.0 reduce-scatter.2.cloned.1.call-start
  178.4 0.7 fusion.28
  179.1 47.1 %all-gather.12 = f32[8192,4]{0,1:T(4,128)S(1)} all-gather(f32[256,4]{0,1:T(4,128)S(1)} %fusion.28), channel_id=14, replica_groups=mesh['sp_0'=8,'sp_1'=4,'sp_2'=2,'tp'=4] {'sp_0','sp_1'}, dimensions={0}, use_global_device_ids=true | all-gather | bytes 135168 | tf_op jit(solution)/shard_map/all_gather | solution.py:25
  226.2 2.0 all-gather.13
  228.2 0.2 copy.37
  228.4 0.3 reshape_reshape.19
  228.7 0.1 copy.38
  228.9 0.3 reduce-window.6
  229.1 0.3 reduce-window.9
  229.5 0.1 copy.39
  229.6 0.2 copy.49
  229.8 49.4 %all_gather.127 = bf16[1024,256]{1,0:T(8,128)(2,1)S(1)} all-gather(bf16[16,256]{1,0:T(8,128)(2,1)} %param.16), channel_id=1, replica_groups=mesh['sp_0'=8,'sp_1'=4,'sp_2'=2,'tp'=4] {'sp_0','sp_1','sp_2'}, dimensions={0}, use_global_device_ids=true | all-gather | bytes 532480 | tf_op jit(solution)/shard_map/all_gather | solution.py:77
  279.3 4.5 %iota_compare_fusion = pred[256,16384]{1,0:T(8,128)(4,1)} fusion(s32[256]{0:T(256)S(1)} %iota_add_fusion), kind=kLoop, calls=%fused_computation.12 | loop fusion | flops 4194304 | bytes 4195328 | tf_op jit(solution)/shard_map/le | solution.py:110
  283.8 0.0 all-gather.18.cloned.1.call-done
  283.8 30.7 %fusion.2 = (f32[4,256]{1,0:T(4,128)S(1)}, f32[4,256,16384]{2,1,0:T(8,128)}) fusion(f32[4,16384]{1,0:T(4,128)S(1)} %bitcast.75, f32[4,256]{1,0:T(4,128)S(1)} %constant_dynamic-slice_fusion, pred[256,16384]{1,0:T(8,128)(4,1)} %iota_compare_fusion, bf16[256,4,64]{0,2,1:T(8,128)(2,1)S(1)} %bitcast.99, bf16[16384,4,64]{0,2,1:T(8,128)(2,1)} %all-gather.18.cloned.1.call-done), kind=kOutput, calls=%fused_computation.4 | convolution fusion | flops 2231368704 | bytes 80093184 | tf_op jit(solution)/shard_map/qhd,khd->hqk/dot_general | solution.py:105
  314.5 31.7 %fusion = f32[4,256]{1,0:T(4,128)S(1)} fusion(f32[4,256,16384]{2,1,0:T(8,128)} %get-tuple-element.13, f32[4,256]{1,0:T(4,128)S(1)} %get-tuple-element.9, f32[4,16384]{1,0:T(4,128)S(1)} %bitcast.76, f32[4,256]{1,0:T(4,128)S(1)} %constant_dynamic-slice_fusion, pred[256,16384]{1,0:T(8,128)(4,1)} %iota_compare_fusion), kind=kLoop, calls=%fused_computation.2 | loop fusion | flops 117439488 | bytes 71577600 | tf_op jit(solution)/shard_map/reduce_sum | solution.py:115
  346.1 2.7 all-gather.20.cloned.1.call-done
  348.9 0.0 copy-start
  348.9 29.7 %fusion.21 = bf16[256,4,64]{0,2,1:T(8,128)(2,1)S(1)} fusion(bf16[16384,4,64]{0,2,1:T(8,128)(2,1)} %all-gather.20.cloned.1.call-done, f32[4,256,16384]{2,1,0:T(8,128)} %get-tuple-element.13, f32[4,256]{1,0:T(4,128)S(1)} %get-tuple-element.9, f32[4,16384]{1,0:T(4,128)S(1)} %bitcast.77, f32[4,256]{1,0:T(4,128)S(1)} %constant_dynamic-slice_fusion, ...), kind=kOutput, calls=%fused_computation.25 | convolution fusion | flops 2248343552 | bytes 80101376 | tf_op jit(solution)/shard_map/hqk,khd->hqd/dot_general | solution.py:116
  378.5 1.2 convolution_convert_fusion
  379.7 0.0 reduce-scatter.2.cloned.1.call-update
  379.7 24.9 %reduce-scatter.2.cloned.1.call-done = bf16[64,1024]{1,0:T(8,128)(2,1)} async-done(((bf16[256,1024]{1,0:T(8,128)(2,1)}), bf16[64,1024]{1,0:T(8,128)(2,1)}) %reduce-scatter.2.cloned.1.call-update) | async-done | bytes 131088 | tf_op jit(solution)/shard_map/reduce_scatter | solution.py:51
  404.6 1.0 fusion.25
  405.7 0.0 copy-done
  405.7 1.7 fusion.27
  (13 shorter events, 0.1 us)
Async XLA Ops:
  6.5 277.2 %all-gather.18.cloned.1.call-start = ((), (), s32[]{:S(2)}) async-start(), calls=%async_computation.1 | async-start | bytes 8519680 | tf_op jit(solution)/shard_map/all_gather | solution.py:43
  177.6 171.3 %all-gather.20.cloned.1.call-start = ((), (), s32[]{:S(2)}) async-start(), calls=%async_computation.2 | async-start | bytes 8519680 | tf_op jit(solution)/shard_map/all_gather | solution.py:43
  178.3 226.3 %reduce-scatter.2.cloned.1.call-start = ((), (), s32[]{:S(2)}) async-start(), calls=%async_computation.3 | async-start | bytes 655360 | tf_op jit(solution)/shard_map/reduce_scatter | solution.py:51
  348.9 56.8 %copy-start = (f32[1024]{0:T(1024)S(1)}, f32[1024]{0:T(1024)}, u32[]{:S(2)}) copy-start(f32[1024]{0:T(1024)} %param.17) | copy-start | bytes 12292
Sparse Core Ops, SparseCore 0:
  177.7 83.5 all-gather.17
  264.0 84.8 all-gather.19
  379.8 24.7 reduce-scatter.1
where the time goes:
time: 417 us; the launch traced here: 414 us
  blocking collectives  265 us (64%)
  matrix products  62.3 us (15%)
  other arithmetic  42.3 us (10%)
  waiting for transfers between devices  28.3 us (7%)
  between operations  13.3 us (3%)
    all_gather x14, blocking collectives, gather_in_order(): parts = lax.all_gather(parts, axes[k])  202 us
    all_gather x1, blocking collectives, shards(): out_weight = lax.all_gather(w_out_t, SP, axis=0, tiled=True)  49.4 us
    reduce_sum x1, other arithmetic, absorb(): new_sum = run_sum * rescale + jnp.sum(shares, axis=-1)  31.7 us
    dot_general x1, matrix products, absorb(): jnp.einsum('qhd,khd->hqk', queries, key_piece, preferred_element_type=jnp...  30.7 us
    dot_general x1, matrix products, absorb(): jnp.einsum('hqk,khd->hqd', shares, value_piece.astype(jnp.float32), preci...  29.7 us
    reduce_scatter x1, waiting for transfers between devices, own_rows(): lax.psum_scatter(sent, axis, scatter_dimension=0, tiled=True)  24.9 us
    all_gather x1, blocking collectives, shards(): all_rows = lax.all_gather(normed, 'tp', axis=0, tiled=True)  13.3 us
  transfers between devices with their start and end apart: 3, of which 2 were waited for; matrix products, arithmetic and copies ran while one was open for 17% of the time, Pallas kernels for 0%

commit v1 on v0

v1 whole, which is shorter than its diff:
```python
import functools
import math

import jax
import jax.numpy as jnp
from jax import lax
from jax.experimental import pallas as pl
from jax.experimental.pallas import tpu as pltpu
from jax.sharding import Mesh
from jax.sharding import PartitionSpec as P

HEAD_DIM = 64
AXES = ("z", "x", "c", "y")
MESH = pl.DeviceIdType.MESH
EPS = 1e-06
LOG2E = 1.4426950408889634
LOW = -1e30
LANES = 128


def rms_norm(floats, gain_row):
    scale_row = lax.rsqrt(jnp.mean(floats * floats, axis=-1, keepdims=True) + EPS)
    return (floats * scale_row * gain_row).astype(jnp.bfloat16)


def log_sigmoid(t):
    u = jnp.exp(-jnp.abs(t))
    series = u * (1.0 - u * (0.5 - u * (1.0 / 3.0 - u * 0.25)))
    return jnp.minimum(t, 0.0) - jnp.where(u < 0.01, series, jnp.log(1.0 + u))


class Links:
    def __init__(self, send_sems, recv_sems, ids):
        self.send_sems, self.recv_sems, self.ids, self.sent = send_sems, recv_sems, ids, []

    def copy(self, key, src, dst, dev):
        at = self.ids.setdefault(key, len(self.ids))
        return pltpu.make_async_remote_copy(
            src_ref=src,
            dst_ref=dst,
            send_sem=self.send_sems.at[at],
            recv_sem=self.recv_sems.at[at],
            device_id=dev,
            device_id_type=MESH,
        )

    def send(self, key, src, dst, dev):
        c = self.copy(key, src, dst, dev)
        c.start()
        self.sent.append(c)

    def recv(self, key, landed, dev):
        self.copy(key, landed, landed, dev).wait_recv()

    def drain(self):
        for c in self.sent:
            c.wait_send()


def kernel(
    dims,
    tokens_ref,
    gain_ref,
    wcat_ref,
    off_ref,
    wo_ref,
    ogain_ref,
    out_ref,
    W,
    XN,
    WO,
    KS,
    VS,
    QS,
    GS,
    GX,
    GP,
    GPR,
    G,
    CUM,
    K,
    VT,
    QT,
    QB,
    M,
    ACC,
    OS,
    AT,
    PT,
    send_sems,
    recv_sems,
):
    Z, X, C, Y = dims
    TB, D = tokens_ref.shape
    GB = TB * Y
    HB = GB // 2
    PR, LW = wcat_ref.shape
    LH = LW // 2
    WC = wo_ref.shape[1]
    z, x, c, y = (lax.axis_index(a) for a in AXES)
    links = Links(send_sems, recv_sems, {})
    UP = Z // 2
    DN = Z - 1 - UP

    def dev(dz=0, dx=0, dc=0, dy=0):
        return {
            "z": lax.rem(z + (dz % Z), Z),
            "x": lax.rem(x + (dx % X), X),
            "c": lax.rem(c + (dc % C), C),
            "y": lax.rem(y + (dy % Y), Y),
        }

    def zrel(d):
        return lax.rem(z + (d % Z), Z)

    def xrel(d):
        return lax.rem(x + (d % X), X)

    def yrel(d):
        return lax.rem(y + (d % Y), Y)

    co = 1 - c
    plane = [(dx, dy) for dx in range(X) for dy in range(Y) if (dx, dy) != (0, 0)]

    barrier = pltpu.get_barrier_semaphore()
    greeted = (
        [dict(dx=dx, dy=dy) for dx, dy in plane]
        + [dict(dx=dx, dc=1) for dx in range(X)]
        + [dict(dz=d) for d in range(1, Z)]
    )
    for g in greeted:
        pl.semaphore_signal(barrier, inc=1, device_id=dev(**g), device_id_type=MESH)
    pl.semaphore_wait(barrier, len(greeted))

    def w_rows(zz, xx, cc):
        return pl.ds(pl.multiple_of(((zz * X + xx) * C + cc) * PR, PR), PR)

    def half(cc):
        return pl.ds(pl.multiple_of(cc * LH, LANES), LH)

    for dx in range(X):
        for dc in range(C):
            if (dx, dc) != (0, 0):
                to = half(c if dc == 0 else co)
                links.send(
                    ("wx", dx, dc), wcat_ref.at[:, to], W.at[w_rows(z, x, c), to], dev(dx=dx, dc=dc)
                )
    W[w_rows(z, x, c), half(c)] = wcat_ref[:, half(c)]

    XN[pl.ds(pl.multiple_of(y * TB, TB), TB), :] = rms_norm(
        tokens_ref[...].astype(jnp.float32), gain_ref[...]
    )
    mine = XN.at[pl.ds(pl.multiple_of(y * TB, TB), TB), :]
    for dy in range(1, Y):
        links.send(("tok", dy), mine, mine, dev(dy=dy))

    def wo_block(cc, xx, zz, yy):
        row = ((cc * X + xx) * Z + zz) * PR
        return WO.at[
            pl.ds(pl.multiple_of(row, PR), PR), pl.ds(pl.multiple_of(yy * WC, LANES), WC)
        ]

    def wo_bundle(cc, xx, yy):
        row = (cc * X + xx) * Z * PR
        return WO.at[
            pl.ds(pl.multiple_of(row, PR), Z * PR), pl.ds(pl.multiple_of(yy * WC, LANES), WC)
        ]

    wo_block(c, x, z, y)[...] = wo_ref[...]

    def ring_start(name, views):
        for a, view in enumerate(views(z, c)):
            if UP > 0:
                links.send((name, "up", 1, a), view, view, dev(dz=1))
            if DN > 0:
                links.send((name, "dn", 1, a), view, view, dev(dz=-1))
        for a, view in enumerate(views(z, c)):
            links.send((name, "core", 0, a), view, view, dev(dc=1))

    def ring_step(name, views, k):
        for a in range(len(views(z, c))):
            for way, sign, last in (("up", 1, UP), ("dn", -1, DN)):
                if k <= last:
                    view = views(zrel(-sign * k), c)[a]
                    links.recv((name, way, k, a), view, dev(dz=-sign))
                    if k < last:
                        links.send((name, way, k + 1, a), view, view, dev(dz=sign))
                    links.send((name, "core", -sign * k, a), view, view, dev(dc=1))

    def other_core(name, views, d):
        for a, view in enumerate(views(zrel(d), co)):
            links.recv((name, "core", d, a), view, dev(dc=1))

    PARTS = 2 if LH % (2 * LANES) == 0 else 1

    def w_views(zz, cc):
        rows = pl.ds(pl.multiple_of(zz * X * C * PR, X * C * PR), X * C * PR)
        step = LH // PARTS
        return [
            W.at[rows, pl.ds(pl.multiple_of(cc * LH + p * step, LANES), step)] for p in range(PARTS)
        ]

    for dx in range(X):
        for dc in range(C):
            if (dx, dc) != (0, 0):
                sx, sc = xrel(-dx), (c if dc == 0 else co)
                links.recv(("wx", dx, dc), W.at[w_rows(z, sx, sc), half(c)], dev(dx=-dx, dc=dc))
    ring_start("w", w_views)
    for d in range(1, Z):
        links.send(("woz", d), wo_ref, wo_block(c, x, z, y), dev(dz=d))
    for k in range(1, UP + 1):
        ring_step("w", w_views, k)
    for d in [0] + list(range(1, DN + 1)) + [-k for k in range(1, UP + 1)]:
        other_core("w", w_views, d)
    for dy in range(1, Y):
        landed = XN.at[pl.ds(pl.multiple_of(yrel(-dy) * TB, TB), TB), :]
        links.recv(("tok", dy), landed, dev(dy=-dy))

    rows = XN[...]
    k_all = jnp.dot(rows, W[:, WC : 2 * WC], preferred_element_type=jnp.float32)
    for h in range(X):
        kh = k_all[:, h * HEAD_DIM : (h + 1) * HEAD_DIM]
        KS[h] = jnp.concatenate([kh[:HB], kh[HB:]], axis=1).astype(jnp.bfloat16)
    v_all = jnp.dot(rows, W[:, 2 * WC : 3 * WC], preferred_element_type=jnp.float32).T
    for h in range(X):
        vh = v_all[h * HEAD_DIM : (h + 1) * HEAD_DIM].astype(jnp.bfloat16)
        VS[h, 0] = vh[:, :HB]
        VS[h, 1] = vh[:, HB:]
    gates = jnp.dot(rows, W[:, 3 * WC : 3 * WC + LANES], preferred_element_type=jnp.float32)
    gates = gates.T[:8]
    head_row = lax.broadcasted_iota(jnp.int32, gates.shape, 0)
    offset = jnp.zeros_like(gates)
    for h in range(X):
        offset = jnp.where(head_row == h, off_ref[h], offset)
    GS[...] = log_sigmoid(gates + offset + math.log(GB * Z * X * C))

    def slot(cc, zz, xx):
        return ((cc * Z + zz) * X + xx) * HB

    def k_block(cc, zz, xx):
        return K.at[pl.ds(pl.multiple_of(slot(cc, zz, xx), LANES), HB), :]

    def v_block(p, cc, zz, xx):
        return VT.at[p, 0:HEAD_DIM, pl.ds(pl.multiple_of(slot(cc, zz, xx), LANES), HB)]

    for dx in range(1, X):
        to = dev(dx=dx)
        links.send(("g", dx), GS, GX.at[x], to)
        links.send(("k", dx), KS.at[xrel(dx)], k_block(c, z, x), to)
        for p in range(2):
            links.send(("v", p, dx), VS.at[xrel(dx), p], v_block(p, c, z, x), to)
    q_all = jnp.dot(rows, W[:, 0:WC], preferred_element_type=jnp.float32)
    q_all = q_all.astype(jnp.bfloat16).astype(jnp.float32) * (HEAD_DIM**-0.5 * LOG2E)
    q_all = q_all.T
    for h in range(X):
        QS[h] = q_all[h * HEAD_DIM : (h + 1) * HEAD_DIM].astype(jnp.bfloat16)
    for dx in range(1, X):
        links.send(("q", dx), QS.at[xrel(dx)], QT.at[x], dev(dx=dx))
    GX[x] = GS[...]
    k_block(c, z, x)[...] = KS[x]
    for p in range(2):
        v_block(p, c, z, x)[...] = VS[x, p]
    QT[x] = QS[x]

    QB[...] = jnp.zeros_like(QB)
    VT[:, HEAD_DIM:, :] = jnp.ones((2, VT.shape[1] - HEAD_DIM, VT.shape[2]), jnp.bfloat16)
    M[...] = jnp.full(M.shape, LOW, jnp.float32)
    ACC[...] = jnp.zeros_like(ACC)

    def my_row(block):
        row = lax.broadcasted_iota(jnp.int32, block.shape, 0)
        return row

    for dx in range(1, X):
        links.recv(("g", dx), GX.at[xrel(-dx)], dev(dx=-dx))
    row8 = lax.broadcasted_iota(jnp.int32, (8, GB), 0)
    own_gates = jnp.zeros((8, GB), jnp.float32)
    for sx in range(X):
        picked = jnp.sum(jnp.where(row8 == x, GX[sx], 0.0), axis=0, keepdims=True)
        own_gates = jnp.where(row8 == sx, picked, own_gates)
    GP[...] = own_gates
    links.send(("gp",), GP, GPR, dev(dc=1))

    for dx in range(1, X):
        sx = xrel(-dx)
        links.recv(("k", dx), k_block(c, z, sx), dev(dx=-dx))
        for p in range(2):
            links.recv(("v", p, dx), v_block(p, c, z, sx), dev(dx=-dx))

    def kv_views(cc, zz):
        at = pl.multiple_of(slot(cc, zz, 0), LANES)
        return [
            K.at[pl.ds(at, X * HB), :],
            VT.at[0, 0:HEAD_DIM, pl.ds(at, X * HB)],
            VT.at[1, 0:HEAD_DIM, pl.ds(at, X * HB)],
        ]

    def kv(zz, cc):
        return kv_views(cc, zz)

    ring_start("kv", kv)

    links.recv(("gp",), GPR, dev(dc=1))
    theirs = GPR[...]
    chip_gates = jnp.zeros((8, GB), jnp.float32)
    for sx in range(X):
        a, b = own_gates[sx : sx + 1], theirs[sx : sx + 1]
        chip_gates = jnp.where(row8 == 2 * sx, jnp.where(c == 0, a, b), chip_gates)
        chip_gates = jnp.where(row8 == 2 * sx + 1, jnp.where(c == 0, b, a), chip_gates)
    G[z] = chip_gates
    for d in range(1, Z):
        links.send(("gz", d), G.at[z], G.at[z], dev(dz=d))
    for dx in range(1, X):
        links.recv(("q", dx), QT.at[xrel(-dx)], dev(dx=-dx))
    for sx in range(X):
        QB[sx, 0:HEAD_DIM, 0:GB] = QT[sx]
        QB[sx, HEAD_DIM:, GB:] = QT[sx]
    for d in range(1, Z):
        links.recv(("woz", d), wo_block(c, x, zrel(-d), y), dev(dz=-d))
    for dx, dy in plane:
        own = wo_bundle(c, x, y)
        links.send(("woxy", dx, dy), own, own, dev(dx=dx, dy=dy))
    links.send(("woc", 0, 0), wo_bundle(c, x, y), wo_bundle(c, x, y), dev(dc=1))

    for d in range(1, Z):
        links.recv(("gz", d), G.at[zrel(-d)], dev(dz=-d))
    cum = G[...].reshape(Z * 8, GB)
    lane = lax.broadcasted_iota(jnp.int32, cum.shape, 1)
    step = 1
    while step < GB:
        cum = cum + jnp.where(lane >= step, pltpu.roll(cum, step, 1), 0.0)
        step *= 2
    total = jnp.broadcast_to(cum[:, GB - 1 :], (Z * 8, LANES))
    row = lax.broadcasted_iota(jnp.int32, total.shape, 0)
    before = jnp.where(row >= 1, pltpu.roll(total, 1, 0), 0.0)
    step = 1
    while step < Z * 8:
        before = before + jnp.where(row >= step, pltpu.roll(before, step, 0), 0.0)
        step *= 2
    cum = (cum + before[:, 0:1]) * LOG2E
    CUM[...] = cum.reshape(Z, 8, GB)

    cum_here = CUM[z]
    cum_q = [
        jnp.sum(jnp.where(row8 == 2 * sx + c, cum_here, 0.0), axis=0, keepdims=True)
        for sx in range(X)
    ]

    def key_bias(zz, cc):
        block = CUM[zz]
        block = jnp.where(cc == 0, block, pltpu.roll(block, 7, 0))
        both = jnp.concatenate([block[:, :HB], block[:, HB:]], axis=0)
        both = jnp.concatenate([both, jnp.zeros((LANES - 16, HB), jnp.float32)], axis=0)
        return both.T

    def chunk(bias, at, pair, tiles, mask):
        at = pl.multiple_of(at + pair * 2 * HB, 2 * HB)
        keys = K[pl.ds(at, 2 * HB), :]
        v0 = VT[0, :, pl.ds(at, 2 * HB)]
        v1 = VT[1, :, pl.ds(at, 2 * HB)]
        b0, b1 = bias
        for t in tiles:
            s = jnp.dot(keys, QB[t], preferred_element_type=jnp.float32)
            s0, s1 = s[:, :GB] - b0, s[:, GB:] - b1
            if mask is not None:
                s0, s1 = mask(s0, 0, t), mask(s1, 1, t)
            old = M[t]
            best = jnp.maximum(jnp.max(s0, axis=0, keepdims=True), jnp.max(s1, axis=0, keepdims=True))
            new = jnp.maximum(old, best + cum_q[t])
            rescale = jnp.exp2(old - new)
            shift = new - cum_q[t]
            p0 = jnp.exp2(s0 - shift).astype(jnp.bfloat16)
            p1 = jnp.exp2(s1 - shift).astype(jnp.bfloat16)
            M[t] = new
            ACC[t] = (
                ACC[t] * rescale
                + jnp.dot(v0, p0, preferred_element_type=jnp.float32)
                + jnp.dot(v1, p1, preferred_element_type=jnp.float32)
            )

    def columns(table, pair):
        even, odd = 4 * pair, 4 * pair + 2
        b0 = jnp.concatenate([table[:, even : even + 1], table[:, odd : odd + 1]], axis=0)
        b1 = jnp.concatenate([table[:, 8 + even : 9 + even], table[:, 8 + odd : 9 + odd]], axis=0)
        return b0, b1

    def past(zz, cc):
        table = key_bias(zz, cc)
        for pair in range(X // 2):
            chunk(columns(table, pair), slot(cc, zz, 0), pair, range(X), None)

    def present(cc):
        table = key_bias(z, cc)
        for pair in range(X // 2):

            def mask(s, which, t, pair=pair):
                r = lax.broadcasted_iota(jnp.int32, s.shape, 0)
                first = 2 * (2 * pair) + cc
                key = jnp.where(r < HB, first * GB + r, (first + 2) * GB + r - HB) + which * HB
                query = (2 * t + c) * GB + lax.broadcasted_iota(jnp.int32, s.shape, 1)
                return jnp.where(key <= query, s, LOW)

            full = [t for t in range(X) if t > 2 * pair + 1]
            cut = [t for t in range(X) if 2 * pair <= t <= 2 * pair + 1]
            bias = columns(table, pair)
            chunk(bias, slot(cc, z, 0), pair, cut, mask)
            if full:
                chunk(bias, slot(cc, z, 0), pair, full, None)

    present_own = functools.partial(present, c)

    def both_cores(zz):
        @pl.loop(0, 2)
        def _(i):
            past(zz, jnp.where(i == 0, c, co))

    present_own()
    other_core("kv", kv, 0)
    present(co)
    for k in range(1, UP + 1):
        ring_step("kv", kv, k)
        other_core("kv", kv, -k)
        if k <= DN:
            other_core("kv", kv, k)

        @pl.when(z - k >= 0)
        def _():
            both_cores(zrel(-k))

        if k <= DN:

            @pl.when(z + k >= Z)
            def _():
                both_cores(zrel(k))

    for dx, dy in plane:
        theirs = wo_bundle(c, xrel(-dx), yrel(-dy))
        links.recv(("woxy", dx, dy), theirs, dev(dx=-dx, dy=-dy))
        links.send(("woc", dx, dy), theirs, theirs, dev(dc=1))

    for t in range(X):
        acc = ACC[t]
        o = (acc[:HEAD_DIM] / acc[HEAD_DIM : HEAD_DIM + 1]).astype(jnp.bfloat16)
        for yy in range(Y):
            OS[t, yy, :, 0:TB] = o[:, yy * TB : (yy + 1) * TB]

    def at_rows(xx, yy):
        return AT.at[pl.ds(pl.multiple_of((yy * X + xx) * HEAD_DIM, HEAD_DIM), HEAD_DIM), :]

    for dx, dy in plane:
        links.send(("o", dx, dy), OS.at[xrel(dx), yrel(dy)], at_rows(x, y), dev(dx=dx, dy=dy))
    at_rows(x, y)[...] = OS[x, y]
    for dx in range(X):
        for dy in range(Y):
            theirs = wo_bundle(co, xrel(-dx), yrel(-dy))
            links.recv(("woc", dx, dy), theirs, dev(dc=1))
    for dx, dy in plane:
        links.recv(("o", dx, dy), at_rows(xrel(-dx), yrel(-dy)), dev(dx=-dx, dy=-dy))

    attended = AT[...]
    for cc in range(C):
        for xx in range(X):
            block = (cc * X + xx) * Z * PR
            part = jnp.dot(
                WO[block : block + Z * PR, :], attended, preferred_element_type=jnp.float32
            )
            for zz in range(Z):
                to = ((zz * X + xx) * C + cc) * PR
                PT[to : to + PR, :] = part[zz * PR : (zz + 1) * PR]
    out_ref[...] = rms_norm(PT[...].T[:TB], ogain_ref[...])
    links.drain()


def layer(dims, tokens, norm_gain, w_query, w_key, w_value, w_forget, forget_offset, w_out_t, out_gain):
    Z, X, C, Y = dims
    TB, D = tokens.shape
    PR, WC = w_query.shape
    GB = TB * Y
    HB = GB // 2
    LW = -(-(3 * WC + LANES) // (2 * LANES)) * 2 * LANES
    pad = jnp.zeros((PR, LW - 3 * WC - w_forget.shape[1]), jnp.bfloat16)
    wcat = jnp.concatenate([w_query, w_key, w_value, w_forget, pad], axis=1)
    keys = Z * X * C * HB
    UP = Z // 2
    n_sems = (
        X * C + Y + 4 * Z + 2 * Z * 3 + 2 * Z * 3 + 6 * X + 2 * Z + 3 * X * Y + 16
    )
    vmem, smem = pl.BlockSpec(memory_space=pltpu.VMEM), pl.BlockSpec(memory_space=pltpu.SMEM)
    bf16, f32 = jnp.bfloat16, jnp.float32
    scratch = [
        pltpu.VMEM((D, LW), bf16),
        pltpu.VMEM((GB, D), bf16),
        pltpu.VMEM((D, D), bf16),
        pltpu.VMEM((X, HB, LANES), bf16),
        pltpu.VMEM((X, 2, HEAD_DIM, HB), bf16),
        pltpu.VMEM((X, HEAD_DIM, GB), bf16),
        pltpu.VMEM((8, GB), f32),
        pltpu.VMEM((X, 8, GB), f32),
        pltpu.VMEM((8, GB), f32),
        pltpu.VMEM((8, GB), f32),
        pltpu.VMEM((Z, 8, GB), f32),
        pltpu.VMEM((Z, 8, GB), f32),
        pltpu.VMEM((keys, LANES), bf16),
        pltpu.VMEM((2, HEAD_DIM + 16, keys), bf16),
        pltpu.VMEM((X, HEAD_DIM, GB), bf16),
        pltpu.VMEM((X, LANES, 2 * GB), bf16),
        pltpu.VMEM((X, 1, GB), f32),
        pltpu.VMEM((X, HEAD_DIM + 16, GB), f32),
        pltpu.VMEM((X, Y, HEAD_DIM, LANES), bf16),
        pltpu.VMEM((D, LANES), bf16),
        pltpu.VMEM((D, LANES), f32),
        pltpu.SemaphoreType.DMA((n_sems,)),
        pltpu.SemaphoreType.DMA((n_sems,)),
    ]
    return pl.pallas_call(
        functools.partial(kernel, dims),
        out_shape=jax.ShapeDtypeStruct((TB, D), bf16),
        in_specs=[vmem, vmem, vmem, smem, vmem, vmem],
        out_specs=vmem,
        scratch_shapes=scratch,
        compiler_params=pltpu.CompilerParams(
            collective_id=0, has_side_effects=True, vmem_limit_bytes=56 * 1024 * 1024
        ),
    )(tokens, norm_gain.reshape(1, D), wcat, forget_offset, w_out_t, out_gain.reshape(1, D))


def sharded(mesh, dims):
    finer = Mesh(mesh.devices.reshape(*dims), AXES)
    sp = ("z", "x", "c")
    return jax.shard_map(
        functools.partial(layer, dims),
        mesh=finer,
        in_specs=(
            P(AXES, None),
            P(),
            P(sp, "y"),
            P(sp, "y"),
            P(sp, "y"),
            P(sp, "y"),
            P("y"),
            P(sp, "y"),
            P(),
        ),
        out_specs=P(AXES, None),
        check_vma=False,
    )


def solution(mesh):
    return sharded(mesh, (8, 4, 2, mesh.shape["tp"]))
```

time: 417 us -> 112 us (0.27)
  blocking collectives: 265 us -> 0 us
  Pallas kernels: 0 us -> 108 us
  matrix products: 62.3 us -> 0 us
  other arithmetic: 42.3 us -> 0 us
  waiting for transfers between devices: 28.3 us -> 0 us
  between operations: 13.3 us -> 0.02 us
    all_gather x16 -> x0, blocking collectives: 265 us -> none  [the longest x14 202 us: gather_in_order(): parts = lax.all_gather(parts, axes[k])]
    pallas_call x0 -> x1, Pallas kernels: none -> 108 us  [layer(): pl.pallas_call(functools.partial(kernel, dims), out_shape=jax.ShapeDtypeS...]
    dot_general x4 -> x0, matrix products: 62.3 us -> none  [the longest x1 30.7 us: absorb(): jnp.einsum('qhd,khd->hqk', queries, key_piece, preferred_element_type=jnp...]
    reduce_sum x3 -> x0, other arithmetic: 33.7 us -> none  [the longest x1 31.7 us: absorb(): new_sum = run_sum * rescale + jnp.sum(shares, axis=-1)]
    reduce_scatter x1 -> x0, waiting for transfers between devices: 24.9 us -> none  [own_rows(): lax.psum_scatter(sent, axis, scatter_dimension=0, tiled=True)]
    le x1 -> x0, other arithmetic: 4.47 us -> none  [absorb(): allowed = (key_pos[None, :] <= query_pos[:, None])[None]]
  transfers between devices with their start and end apart: 3 -> 0, of which waited for: 2 -> 0; matrix products, arithmetic and copies ran while one was open for 17% -> 0% of each run, Pallas kernels for 0% -> 0%
where the time goes in v1:
time: 112 us
  Pallas kernels  108 us (96%)
  local copies, waits for them, and re-layouts  3.77 us (3%)
    pallas_call x1, Pallas kernels, layer(): pl.pallas_call(functools.partial(kernel, dims), out_shape=jax.ShapeDtypeS...  108 us
    unnamed x6, local copies, waits for them, and re-layouts  2.37 us

profile of v1, /device:TPU:224, one launch (start us, length us, event | category | flops | bytes accessed | tf_op | source)
XLA Modules:
  0.0 111.7 jit_solution(1069541319443010741)
XLA Ops:
  0.0 0.0 copy-start.1
  0.0 0.0 copy-start
  0.0 0.8 copy.10
  0.8 0.0 copy-done.1
  0.8 0.0 copy-done
  0.8 1.4 %concatenate.3.wcat_ref = bf16[16,1024]{1,0:T(8,128)(2,1)} concatenate(bf16[16,256]{1,0:T(8,128)(2,1)S(1)} %copy-done, bf16[16,256]{1,0:T(8,128)(2,1)S(1)} %copy-done.1, bf16[16,256]{1,0:T(8,128)(2,1)} %param.13, bf16[16,4]{1,0:T(8,128)(2,1)S(1)} %copy.10, bf16[16,252]{1,0:T(8,128)(2,1)S(1)} %broadcast_in_dim.3), dimensions={1} | concatenate | bytes 65536 | tf_op jit(solution)/shard_map/concatenate | solution.py:482
  2.2 107.9 %shard_map.91 = bf16[64,1024]{1,0:T(8,128)(2,1)} custom-call(bf16[64,1024]{1,0:T(8,128)(2,1)} %tokens_ref.1, f32[1,1024]{1,0:T(1,128)} %bitcast.2, bf16[16,1024]{1,0:T(8,128)(2,1)} %concatenate.3.wcat_ref, f32[4]{0:T(128)} %off_ref.1, bf16[16,256]{1,0:T(8,128)(2,1)} %wo_ref.1, f32[1,1024]{1,0:T(1,128)} %bitcast.3), custom_call_target="tpu_custom_call" | custom-call | tf_op jit(solution)/shard_map/pallas_call | solution.py:515
  110.2 1.6 %copy.12 = bf16[64,1024]{1,0:T(8,128)(2,1)} copy(bf16[64,1024]{1,0:T(8,128)(2,1)} %shard_map.91) | data formatting | bytes 262144
  (1 shorter events, 0.0 us)
Async XLA Ops:
  0.0 0.8 copy-start.1
  0.0 0.8 copy-start

commit v2 on v1

v2 whole, which is shorter than its diff:
```python
import functools
import math

import jax
import jax.numpy as jnp
from jax import lax
from jax.experimental import pallas as pl
from jax.experimental.pallas import tpu as pltpu
from jax.sharding import Mesh
from jax.sharding import PartitionSpec as P

HEAD_DIM = 64
AXES = ("z", "x", "c", "y")
MESH = pl.DeviceIdType.MESH
EPS = 1e-06
LOG2E = 1.4426950408889634
LOW = -1e30
LANES = 128


def rms_norm(floats, gain_row):
    scale_row = lax.rsqrt(jnp.mean(floats * floats, axis=-1, keepdims=True) + EPS)
    return (floats * scale_row * gain_row).astype(jnp.bfloat16)


def log_sigmoid(t):
    u = jnp.exp(-jnp.abs(t))
    series = u * (1.0 - u * (0.5 - u * (1.0 / 3.0 - u * 0.25)))
    return jnp.minimum(t, 0.0) - jnp.where(u < 0.01, series, jnp.log(1.0 + u))


class Links:
    def __init__(self, send_sems, recv_sems, ids):
        self.send_sems, self.recv_sems, self.ids, self.sent = send_sems, recv_sems, ids, []

    def copy(self, key, src, dst, dev):
        at = self.ids.setdefault(key, len(self.ids))
        return pltpu.make_async_remote_copy(
            src_ref=src,
            dst_ref=dst,
            send_sem=self.send_sems.at[at],
            recv_sem=self.recv_sems.at[at],
            device_id=dev,
            device_id_type=MESH,
        )

    def send(self, key, src, dst, dev):
        c = self.copy(key, src, dst, dev)
        c.start()
        self.sent.append(c)

    def recv(self, key, landed, dev):
        self.copy(key, landed, landed, dev).wait_recv()

    def drain(self):
        for c in self.sent:
            c.wait_send()


def kernel(
    dims,
    tokens_ref,
    gain_ref,
    wq_ref,
    wk_ref,
    wv_ref,
    wf_ref,
    off_ref,
    wo_ref,
    ogain_ref,
    out_ref,
    W,
    XN,
    WO,
    KS,
    VS,
    QS,
    GS,
    GX,
    GP,
    GPR,
    G,
    CUM,
    K,
    VT,
    QT,
    QB,
    M,
    ACC,
    OS,
    AT,
    PT,
    SC,
    PB,
    send_sems,
    recv_sems,
):
    Z, X, C, Y = dims
    TB, D = tokens_ref.shape
    GB = TB * Y
    HB = GB // 2
    PR, WC = wo_ref.shape
    LW = W.shape[2]
    z, x, c, y = (lax.axis_index(a) for a in AXES)
    links = Links(send_sems, recv_sems, {})

    def dev(dz=0, dx=0, dc=0, dy=0):
        return {
            "z": lax.rem(z + (dz % Z), Z),
            "x": lax.rem(x + (dx % X), X),
            "c": lax.rem(c + (dc % C), C),
            "y": lax.rem(y + (dy % Y), Y),
        }

    def zrel(d):
        return lax.rem(z + (d % Z), Z)

    def xrel(d):
        return lax.rem(x + (d % X), X)

    def yrel(d):
        return lax.rem(y + (d % Y), Y)

    co = 1 - c
    plane = [(dx, dy) for dx in range(X) for dy in range(Y) if (dx, dy) != (0, 0)]
    far_first = sorted(range(1, Z), key=lambda d: -min(d, Z - d))
    near_first = [0] + far_first[::-1]
    x_near, y_near = ([1] if n == 2 else [1, -1] for n in (X, Y))

    barrier = pltpu.get_barrier_semaphore()
    greeted = (
        [dict(dx=dx, dy=dy) for dx, dy in plane] + [dict(dc=1)] + [dict(dz=d) for d in range(1, Z)]
    )
    for g in greeted:
        pl.semaphore_signal(barrier, inc=1, device_id=dev(**g), device_id_type=MESH)

    def w_rows(xx, cc):
        return pl.ds(pl.multiple_of((xx * C + cc) * PR, PR), PR)

    KV, QF = (0, 2 * WC), (2 * WC, LW)
    mine = w_rows(x, c)
    W[z, mine, 0:WC] = wk_ref[...]
    W[z, mine, WC : 2 * WC] = wv_ref[...]
    W[z, mine, 2 * WC : 3 * WC] = wq_ref[...]
    W[z, mine, 3 * WC :] = jnp.zeros((PR, LANES), jnp.bfloat16)
    W[z, mine, 3 * WC : 3 * WC + wf_ref.shape[1]] = wf_ref[...]

    def t_rows(yy, lo=0, count=TB):
        return XN.at[pl.ds(pl.multiple_of(yy * TB + lo, 32), count), :]

    t_rows(y)[...] = rms_norm(tokens_ref[...].astype(jnp.float32), gain_ref[...])

    def wo_block(cc, xx, zz, yy):
        row = ((cc * X + xx) * Z + zz) * PR
        return WO.at[
            pl.ds(pl.multiple_of(row, PR), PR), pl.ds(pl.multiple_of(yy * WC, LANES), WC)
        ]

    def wo_bundle(cc, xx, yy):
        row = (cc * X + xx) * Z * PR
        return WO.at[
            pl.ds(pl.multiple_of(row, PR), Z * PR), pl.ds(pl.multiple_of(yy * WC, LANES), WC)
        ]

    wo_block(c, x, z, y)[...] = wo_ref[...]
    pl.semaphore_wait(barrier, len(greeted))

    def w_unit(d, xx, cc, lanes):
        return W.at[zrel(d), w_rows(xx, cc), lanes[0] : lanes[1]]

    def w_bundle(xx, cc, lanes):
        return W.at[:, w_rows(xx, cc), lanes[0] : lanes[1]]

    def halves(lanes):
        middle = lanes[0] + WC
        return (lanes[0], middle), (middle, lanes[1])

    def along_x(d, lanes):
        for dx in x_near:
            unit = w_unit(d, x, c, lanes)
            links.send(("x1", lanes, d, dx), unit, unit, dev(dx=dx))

    def z_stage(lanes):
        for d in near_first:
            if d != 0:
                links.recv(("wz", lanes, d), w_unit(-d, x, c, lanes), dev(dz=-d))
            along_x(-d % Z, lanes)
        own = w_bundle(x, c, lanes)
        links.send(("wc", lanes, 0), own, own, dev(dc=1))

    def x_stage(lanes):
        for d in near_first:
            for dx, part in zip(x_near, halves(lanes)):
                links.recv(("x1", lanes, -d % Z, dx), w_unit(-d, xrel(-dx), c, lanes), dev(dx=-dx))
                if X > 2:
                    unit = w_unit(-d, xrel(-dx), c, part)
                    links.send(("x2", lanes, -d % Z, dx), unit, unit, dev(dx=dx))
        for dx in x_near:
            theirs = w_bundle(xrel(-dx), c, lanes)
            links.send(("wc", lanes, dx % X), theirs, theirs, dev(dc=1))

    def x_last(lanes):
        if X > 2:
            for d in near_first:
                for dx, part in zip(x_near, halves(lanes)):
                    unit = w_unit(-d, xrel(2), c, part)
                    links.recv(("x2", lanes, -d % Z, dx), unit, dev(dx=-dx))
            theirs = w_bundle(xrel(2), c, lanes)
            links.send(("wc", lanes, 2), theirs, theirs, dev(dc=1))

    def core_last(lanes):
        for dx in range(X):
            links.recv(("wc", lanes, dx), w_bundle(xrel(-dx), co, lanes), dev(dc=1))

    for lanes in (KV, QF):
        for d in far_first:
            unit = w_unit(0, x, c, lanes)
            links.send(("wz", lanes, d), unit, unit, dev(dz=d))
    for dy in y_near:
        links.send(("tok", dy), t_rows(y), t_rows(y), dev(dy=dy))
    for d in far_first:
        links.send(("woz", d), wo_ref, wo_block(c, x, z, y), dev(dz=d))

    QB[...] = jnp.zeros_like(QB)
    VT[:, HEAD_DIM:, :] = jnp.ones((2, VT.shape[1] - HEAD_DIM, VT.shape[2]), jnp.bfloat16)
    M[...] = jnp.full(M.shape, LOW, jnp.float32)
    ACC[...] = jnp.zeros_like(ACC)

    z_stage(KV)
    for dy, lo in zip(y_near, (0, TB // 2)):
        links.recv(("tok", dy), t_rows(yrel(-dy)), dev(dy=-dy))
        if Y > 2:
            part = t_rows(yrel(-dy), lo, TB // 2)
            links.send(("tok2", dy), part, part, dev(dy=dy))
    x_stage(KV)
    z_stage(QF)
    x_last(KV)
    x_stage(QF)
    if Y > 2:
        for dy, lo in zip(y_near, (0, TB // 2)):
            links.recv(("tok2", dy), t_rows(yrel(2), lo, TB // 2), dev(dy=-dy))
    core_last(KV)

    rows = XN[...]

    def project(lo, count):
        weight = W[:, :, lo : lo + count].reshape(D, count)
        return jnp.dot(rows, weight, preferred_element_type=jnp.float32)

    def slot(cc, zz, xx):
        return ((cc * Z + zz) * X + xx) * HB

    def k_block(cc, zz, xx):
        return K.at[pl.ds(pl.multiple_of(slot(cc, zz, xx), LANES), HB), :]

    def v_block(p, cc, zz, xx):
        return VT.at[p, 0:HEAD_DIM, pl.ds(pl.multiple_of(slot(cc, zz, xx), LANES), HB)]

    k_all = project(0, WC)
    for h in range(X):
        kh = k_all[:, h * HEAD_DIM : (h + 1) * HEAD_DIM]
        KS[h] = jnp.concatenate([kh[:HB], kh[HB:]], axis=1).astype(jnp.bfloat16)
    for dx in range(1, X):
        links.send(("k", dx), KS.at[xrel(dx)], k_block(c, z, x), dev(dx=dx))
    v_all = project(WC, WC).T
    for h in range(X):
        vh = v_all[h * HEAD_DIM : (h + 1) * HEAD_DIM].astype(jnp.bfloat16)
        VS[h, 0] = vh[:, :HB]
        VS[h, 1] = vh[:, HB:]
    for dx in range(1, X):
        for p in range(2):
            links.send(("v", p, dx), VS.at[xrel(dx), p], v_block(p, c, z, x), dev(dx=dx))
    k_block(c, z, x)[...] = KS[x]
    for p in range(2):
        v_block(p, c, z, x)[...] = VS[x, p]

    x_last(QF)
    core_last(QF)
    gates = project(3 * WC, LANES).T[:8]
    head_row = lax.broadcasted_iota(jnp.int32, gates.shape, 0)
    offset = jnp.zeros_like(gates)
    for h in range(X):
        offset = jnp.where(head_row == h, off_ref[h], offset)
    GS[...] = log_sigmoid(gates + offset + math.log(GB * Z * X * C))
    for dx in range(1, X):
        links.send(("g", dx), GS, GX.at[x], dev(dx=dx))
    q_all = project(2 * WC, WC)
    q_all = q_all.astype(jnp.bfloat16).astype(jnp.float32) * (HEAD_DIM**-0.5 * LOG2E)
    q_all = q_all.T
    for h in range(X):
        QS[h] = q_all[h * HEAD_DIM : (h + 1) * HEAD_DIM].astype(jnp.bfloat16)
    for dx in range(1, X):
        links.send(("q", dx), QS.at[xrel(dx)], QT.at[x], dev(dx=dx))
    GX[x] = GS[...]
    QT[x] = QS[x]

    UP = DN = Z // 2

    def goes(way, a, k):
        return k < UP or (k == UP and (a == 0) == (way == "up"))

    def kv(zz, cc):
        at = pl.multiple_of(slot(cc, zz, 0), LANES)
        return [
            K.at[pl.ds(at, X * HB), :],
            VT.at[0, 0:HEAD_DIM, pl.ds(at, X * HB)],
            VT.at[1, 0:HEAD_DIM, pl.ds(at, X * HB)],
        ]

    WAYS = (("up", 1), ("dn", -1))

    def ring_start():
        for a, view in enumerate(kv(z, c)):
            for way, sign in WAYS:
                if goes(way, a, 1):
                    links.send((way, 1, a), view, view, dev(dz=sign))
        for a, view in enumerate(kv(z, c)):
            links.send(("core", 0, a), view, view, dev(dc=1))

    def ring_step(k):
        for a in range(3):
            for way, sign in WAYS:
                if goes(way, a, k):
                    view = kv(zrel(-sign * k), c)[a]
                    links.recv((way, k, a), view, dev(dz=-sign))
                    if goes(way, a, k + 1):
                        links.send((way, k + 1, a), view, view, dev(dz=sign))
                    links.send(("core", -sign * k % Z, a), view, view, dev(dc=1))

    def other_core(d):
        for a, view in enumerate(kv(zrel(d), co)):
            links.recv(("core", d % Z, a), view, dev(dc=1))

    for dx in range(1, X):
        sx = xrel(-dx)
        links.recv(("k", dx), k_block(c, z, sx), dev(dx=-dx))
        for p in range(2):
            links.recv(("v", p, dx), v_block(p, c, z, sx), dev(dx=-dx))
    ring_start()

    for dx in range(1, X):
        links.recv(("g", dx), GX.at[xrel(-dx)], dev(dx=-dx))
    row8 = lax.broadcasted_iota(jnp.int32, (8, GB), 0)
    own_gates = jnp.zeros((8, GB), jnp.float32)
    for sx in range(X):
        picked = jnp.sum(jnp.where(row8 == x, GX[sx], 0.0), axis=0, keepdims=True)
        own_gates = jnp.where(row8 == sx, picked, own_gates)
    GP[...] = own_gates
    links.send(("gp",), GP, GPR, dev(dc=1))
    links.recv(("gp",), GPR, dev(dc=1))
    theirs = GPR[...]
    chip_gates = jnp.zeros((8, GB), jnp.float32)
    for sx in range(X):
        a, b = own_gates[sx : sx + 1], theirs[sx : sx + 1]
        chip_gates = jnp.where(row8 == 2 * sx, jnp.where(c == 0, a, b), chip_gates)
        chip_gates = jnp.where(row8 == 2 * sx + 1, jnp.where(c == 0, b, a), chip_gates)
    G[z] = chip_gates
    for d in far_first:
        links.send(("gz", d), G.at[z], G.at[z], dev(dz=d))
    for dx in range(1, X):
        links.recv(("q", dx), QT.at[xrel(-dx)], dev(dx=-dx))
    for sx in range(X):
        QB[sx, 0:HEAD_DIM, 0:GB] = QT[sx]
        QB[sx, HEAD_DIM:, GB:] = QT[sx]
    for d in far_first:
        links.recv(("woz", d), wo_block(c, x, zrel(-d), y), dev(dz=-d))
    own = wo_bundle(c, x, y)
    for dx, dy in plane:
        links.send(("woxy", dx, dy), own, own, dev(dx=dx, dy=dy))
    links.send(("woc", 0, 0), own, own, dev(dc=1))

    def cumulative(block):
        n = block.shape[0]
        lane = lax.broadcasted_iota(jnp.int32, block.shape, 1)
        step = 1
        while step < GB:
            block = block + jnp.where(lane >= step, pltpu.roll(block, step, 1), 0.0)
            step *= 2
        total = jnp.broadcast_to(block[:, GB - 1 :], (n, LANES))
        row = lax.broadcasted_iota(jnp.int32, total.shape, 0)
        before = jnp.where(row >= 1, pltpu.roll(total, 1, 0), 0.0)
        step = 1
        while step < n:
            before = before + jnp.where(row >= step, pltpu.roll(before, step, 0), 0.0)
            step *= 2
        return (block + before[:, 0:1]) * LOG2E

    def query_sums(block):
        return [
            jnp.sum(jnp.where(row8 == 2 * sx + c, block, 0.0), axis=0, keepdims=True)
            for sx in range(X)
        ]

    def key_sums(block, cc):
        block = jnp.where(cc == 0, block, pltpu.roll(block, 7, 0))
        both = jnp.concatenate([block[:, :HB], block[:, HB:]], axis=0)
        both = jnp.concatenate([both, jnp.zeros((LANES - 16, HB), jnp.float32)], axis=0)
        return both.T

    def attend(items, cum_q):
        AHEAD, SOFT = 3, 1
        n_s, n_p = AHEAD - SOFT + 1, SOFT + 1
        best, rescale, loaded = {}, {}, {}

        def prepared(table, at, pair):
            key = (id(table), pair)
            if key not in loaded:
                even, odd = 4 * pair, 4 * pair + 2
                b0 = [table[:, even : even + 1], table[:, odd : odd + 1]]
                b1 = [table[:, 8 + even : 9 + even], table[:, 8 + odd : 9 + odd]]
                start = pl.multiple_of(at + pair * 2 * HB, 2 * HB)
                loaded[key] = jnp.concatenate(b0, axis=0), jnp.concatenate(b1, axis=0), start
            return loaded[key]

        def scores(j):
            table, at, pair, t, mask = items[j]
            b0, b1, start = prepared(table, at, pair)
            s = jnp.dot(K[pl.ds(start, 2 * HB), :], QB[t], preferred_element_type=jnp.float32)
            s0, s1 = s[:, :GB] - b0, s[:, GB:] - b1
            if mask is not None:
                s0, s1 = mask(s0, 0, t), mask(s1, 1, t)
            SC[j % n_s, 0], SC[j % n_s, 1] = s0, s1
            best[j] = jnp.maximum(jnp.max(s0, axis=0, keepdims=True), jnp.max(s1, axis=0, keepdims=True))

        def softmax(j):
            t = items[j][3]
            old = M[t]
            new = jnp.maximum(old, best[j] + cum_q[t])
            rescale[j] = jnp.exp2(old - new)
            M[t] = new
            shift = new - cum_q[t]
            PB[j % n_p, : 2 * HB] = jnp.exp2(SC[j % n_s, 0] - shift).astype(jnp.bfloat16)
            PB[j % n_p, 2 * HB :] = jnp.exp2(SC[j % n_s, 1] - shift).astype(jnp.bfloat16)

        def weigh(j):
            table, at, pair, t, _ = items[j]
            start = prepared(table, at, pair)[2]
            v = jnp.concatenate(
                [VT[0, :, pl.ds(start, 2 * HB)], VT[1, :, pl.ds(start, 2 * HB)]], axis=1
            )
            ACC[t] = ACC[t] * rescale[j] + jnp.dot(
                v, PB[j % n_p], preferred_element_type=jnp.float32
            )

        for j in range(-AHEAD, len(items)):
            if 0 <= j + AHEAD < len(items):
                scores(j + AHEAD)
            if j >= 0:
                weigh(j)
            if 0 <= j + SOFT < len(items):
                softmax(j + SOFT)

    cum_here = cumulative(G[z])
    cum_q_here = query_sums(cum_here)

    @pl.loop(0, 2)
    def _(i):
        cc = jnp.where(i == 0, c, co)

        @pl.when(i == 1)
        def _():
            other_core(0)

        def masked(pair):
            def mask(s, which, t):
                r = lax.broadcasted_iota(jnp.int32, s.shape, 0)
                first = 4 * pair + cc
                key = jnp.where(r < HB, first * GB + r, (first + 2) * GB + r - HB) + which * HB
                query = (2 * t + c) * GB + lax.broadcasted_iota(jnp.int32, s.shape, 1)
                return jnp.where(key <= query, s, LOW)

            return mask

        table = key_sums(cum_here, cc)
        items = [
            (table, slot(cc, z, 0), pair, t, masked(pair) if t <= 2 * pair + 1 else None)
            for pair in range(X // 2)
            for t in range(2 * pair, X)
        ]
        attend(items, cum_q_here)

    for d in far_first:
        links.recv(("gz", d), G.at[zrel(-d)], dev(dz=-d))
    CUM[...] = cumulative(G[...].reshape(Z * 8, GB)).reshape(Z, 8, GB)
    cum_q = query_sums(CUM[z])

    def past(ds):
        @pl.loop(0, 2)
        def _(i):
            cc = jnp.where(i == 0, c, co)

            @pl.when(i == 1)
            def _():
                for d in ds:
                    other_core(d)

            items = []
            for d in ds:
                zz = zrel(d)
                table = key_sums(CUM[zz], cc)
                items += [
                    (table, slot(cc, zz, 0), pair, t, None)
                    for pair in range(X // 2)
                    for t in range(X)
                ]
            attend(items, cum_q)

    def skipped(ds):
        for d in ds:
            other_core(d)

    def wo_forward():
        for dx, dy in plane:
            theirs = wo_bundle(c, xrel(-dx), yrel(-dy))
            links.recv(("woxy", dx, dy), theirs, dev(dx=-dx, dy=-dy))
            links.send(("woc", dx, dy), theirs, theirs, dev(dc=1))

    for k in range(1, UP + 1):
        ring_step(k)
        if k == UP:
            wo_forward()
        both = [-k, k] if k < UP else [-k]
        if k < UP:

            @pl.when(z + k >= Z)
            def _():
                past(both)

            @pl.when((z >= k) & (z + k < Z))
            def _():
                past([-k])
                skipped([k])

        else:

            @pl.when(z >= k)
            def _():
                past(both)

        @pl.when(z < k)
        def _():
            skipped(both)

    for t in range(X):
        acc = ACC[t]
        o = (acc[:HEAD_DIM] / acc[HEAD_DIM : HEAD_DIM + 1]).astype(jnp.bfloat16)
        for yy in range(Y):
            OS[t, yy, :, 0:TB] = o[:, yy * TB : (yy + 1) * TB]

    def at_rows(xx, yy):
        return AT.at[pl.ds(pl.multiple_of((yy * X + xx) * HEAD_DIM, HEAD_DIM), HEAD_DIM), :]

    for dx, dy in plane:
        links.send(("o", dx, dy), OS.at[xrel(dx), yrel(dy)], at_rows(x, y), dev(dx=dx, dy=dy))
    at_rows(x, y)[...] = OS[x, y]
    for dx in range(X):
        for dy in range(Y):
            theirs = wo_bundle(co, xrel(-dx), yrel(-dy))
            links.recv(("woc", dx, dy), theirs, dev(dc=1))
    for dx, dy in plane:
        links.recv(("o", dx, dy), at_rows(xrel(-dx), yrel(-dy)), dev(dx=-dx, dy=-dy))

    attended = AT[...]
    for cc in range(C):
        for xx in range(X):
            block = (cc * X + xx) * Z * PR
            part = jnp.dot(
                WO[block : block + Z * PR, :], attended, preferred_element_type=jnp.float32
            )
            for zz in range(Z):
                to = ((zz * X + xx) * C + cc) * PR
                PT[to : to + PR, :] = part[zz * PR : (zz + 1) * PR]
    out_ref[...] = rms_norm(PT[...].T[:TB], ogain_ref[...])
    links.drain()


def layer(dims, tokens, norm_gain, w_query, w_key, w_value, w_forget, forget_offset, w_out_t, out_gain):
    Z, X, C, Y = dims
    TB, D = tokens.shape
    PR, WC = w_query.shape
    GB = TB * Y
    HB = GB // 2
    LW = 3 * WC + LANES
    keys = Z * X * C * HB
    n_sems = 260
    vmem, smem = pl.BlockSpec(memory_space=pltpu.VMEM), pl.BlockSpec(memory_space=pltpu.SMEM)
    bf16, f32 = jnp.bfloat16, jnp.float32
    scratch = [
        pltpu.VMEM((Z, X * C * PR, LW), bf16),
        pltpu.VMEM((GB, D), bf16),
        pltpu.VMEM((D, D), bf16),
        pltpu.VMEM((X, HB, LANES), bf16),
        pltpu.VMEM((X, 2, HEAD_DIM, HB), bf16),
        pltpu.VMEM((X, HEAD_DIM, GB), bf16),
        pltpu.VMEM((8, GB), f32),
        pltpu.VMEM((X, 8, GB), f32),
        pltpu.VMEM((8, GB), f32),
        pltpu.VMEM((8, GB), f32),
        pltpu.VMEM((Z, 8, GB), f32),
        pltpu.VMEM((Z, 8, GB), f32),
        pltpu.VMEM((keys, LANES), bf16),
        pltpu.VMEM((2, HEAD_DIM + 16, keys), bf16),
        pltpu.VMEM((X, HEAD_DIM, GB), bf16),
        pltpu.VMEM((X, LANES, 2 * GB), bf16),
        pltpu.VMEM((X, 1, GB), f32),
        pltpu.VMEM((X, HEAD_DIM + 16, GB), f32),
        pltpu.VMEM((X, Y, HEAD_DIM, LANES), bf16),
        pltpu.VMEM((D, LANES), bf16),
        pltpu.VMEM((D, LANES), f32),
        pltpu.VMEM((3, 2, 2 * HB, GB), f32),
        pltpu.VMEM((2, 4 * HB, GB), bf16),
        pltpu.SemaphoreType.DMA((n_sems,)),
        pltpu.SemaphoreType.DMA((n_sems,)),
    ]
    return pl.pallas_call(
        functools.partial(kernel, dims),
        out_shape=jax.ShapeDtypeStruct((TB, D), bf16),
        in_specs=[vmem] * 6 + [smem, vmem, vmem],
        out_specs=vmem,
        scratch_shapes=scratch,
        compiler_params=pltpu.CompilerParams(
            collective_id=0, has_side_effects=True, vmem_limit_bytes=56 * 1024 * 1024
        ),
    )(
        tokens,
        norm_gain.reshape(1, D),
        w_query,
        w_key,
        w_value,
        w_forget,
        forget_offset,
        w_out_t,
        out_gain.reshape(1, D),
    )


def sharded(mesh, dims):
    finer = Mesh(mesh.devices.reshape(*dims), AXES)
    sp = ("z", "x", "c")
    return jax.shard_map(
        functools.partial(layer, dims),
        mesh=finer,
        in_specs=(
            P(AXES, None),
            P(),
            P(sp, "y"),
            P(sp, "y"),
            P(sp, "y"),
            P(sp, "y"),
            P("y"),
            P(sp, "y"),
            P(),
        ),
        out_specs=P(AXES, None),
        check_vma=False,
    )


def solution(mesh):
    return sharded(mesh, (8, 4, 2, mesh.shape["tp"]))
```

time: 112 us -> 79.3 us (0.71)
  the two profiles are of different devices: /device:TPU:224 before, /device:TPU:1 now
where the time goes in v2:
time: 79.3 us; the launch traced here: 79.2 us
  Pallas kernels  76.3 us (96%)
  local copies, waits for them, and re-layouts  2.93 us (4%)
    pallas_call x1, Pallas kernels, layer(): pl.pallas_call(functools.partial(kernel, dims), out_shape=jax.ShapeDtypeS...  76.3 us
    unnamed x4, local copies, waits for them, and re-layouts  2.93 us

profile of v2, /device:TPU:1, one launch (start us, length us, event | category | flops | bytes accessed | tf_op | source)
XLA Modules:
  0.0 79.2 jit_solution(3554570916873427194)
XLA Ops:
  0.0 0.0 copy-start
  0.0 0.7 copy-done
  0.7 0.7 copy.10.wf_ref
  1.4 76.3 %shard_map.91 = bf16[64,1024]{1,0:T(8,128)(2,1)} custom-call(bf16[64,1024]{1,0:T(8,128)(2,1)} %tokens_ref.1, f32[1,1024]{1,0:T(1,128)} %bitcast.2, bf16[16,256]{1,0:T(8,128)(2,1)} %wq_ref.1, bf16[16,256]{1,0:T(8,128)(2,1)} %wk_ref.1, bf16[16,256]{1,0:T(8,128)(2,1)} %wv_ref.1, bf16[16,4]{1,0:T(8,128)(2,1)} %copy.10.wf_ref, f32[4]{0:T(128)} %off_ref.1, ...), custom_call_target="tpu_custom_call" | custom-call | tf_op jit(solution)/shard_map/pallas_call | solution.py:615
  77.6 1.6 %copy.12 = bf16[64,1024]{1,0:T(8,128)(2,1)} copy(bf16[64,1024]{1,0:T(8,128)(2,1)} %shard_map.91) | data formatting | bytes 262144
Async XLA Ops:
  0.0 0.7 copy-start

commit v3 on v2

--- a/solution.py
+++ b/solution.py
@@ -92,6 +92,7 @@
     PT,
     SC,
     PB,
+    WO_OWN,
     send_sems,
     recv_sems,
 ):
@@ -137,32 +138,39 @@
     def w_rows(xx, cc):
         return pl.ds(pl.multiple_of((xx * C + cc) * PR, PR), PR)
 
-    KV, QF = (0, 2 * WC), (2 * WC, LW)
+    KVF, Q = (0, 2 * WC + LANES), (2 * WC + LANES, LW)
     mine = w_rows(x, c)
     W[z, mine, 0:WC] = wk_ref[...]
     W[z, mine, WC : 2 * WC] = wv_ref[...]
-    W[z, mine, 2 * WC : 3 * WC] = wq_ref[...]
-    W[z, mine, 3 * WC :] = jnp.zeros((PR, LANES), jnp.bfloat16)
-    W[z, mine, 3 * WC : 3 * WC + wf_ref.shape[1]] = wf_ref[...]
+    W[z, mine, KVF[1] :] = wq_ref[...]
+    PT[0:LANES] = jnp.zeros((LANES, LANES), jnp.float32)
+    PT[0:X, 0:PR] = wf_ref[...].astype(jnp.float32)
+    W[z, mine, 2 * WC : KVF[1]] = PT[0:LANES].T[:PR].astype(jnp.bfloat16)
 
     def t_rows(yy, lo=0, count=TB):
         return XN.at[pl.ds(pl.multiple_of(yy * TB + lo, 32), count), :]
 
     t_rows(y)[...] = rms_norm(tokens_ref[...].astype(jnp.float32), gain_ref[...])
 
+    HALF = HEAD_DIM // 2
+    WH = WC // 2
+
+    def wo_columns(yy):
+        return pl.ds(pl.multiple_of(yy * WH, WH), WH)
+
     def wo_block(cc, xx, zz, yy):
         row = ((cc * X + xx) * Z + zz) * PR
-        return WO.at[
-            pl.ds(pl.multiple_of(row, PR), PR), pl.ds(pl.multiple_of(yy * WC, LANES), WC)
-        ]
+        return WO.at[:, pl.ds(pl.multiple_of(row, PR), PR), wo_columns(yy)]
 
     def wo_bundle(cc, xx, yy):
         row = (cc * X + xx) * Z * PR
-        return WO.at[
-            pl.ds(pl.multiple_of(row, PR), Z * PR), pl.ds(pl.multiple_of(yy * WC, LANES), WC)
-        ]
-
-    wo_block(c, x, z, y)[...] = wo_ref[...]
+        return WO.at[:, pl.ds(pl.multiple_of(row, PR), Z * PR), wo_columns(yy)]
+
+    own_wo = wo_ref[...].astype(jnp.float32)
+    for h in range(2):
+        cols = [own_wo[:, i * HALF : (i + 1) * HALF] for i in range(h, 2 * X, 2)]
+        WO_OWN[h] = jnp.concatenate(cols, axis=1).astype(jnp.bfloat16)
+    wo_block(c, x, z, y)[...] = WO_OWN[...]
     pl.semaphore_wait(barrier, len(greeted))
 
     def w_unit(d, xx, cc, lanes):
@@ -172,7 +180,7 @@
         return W.at[:, w_rows(xx, cc), lanes[0] : lanes[1]]
 
     def halves(lanes):
-        middle = lanes[0] + WC
+        middle = lanes[0] + -(-(lanes[1] - lanes[0]) // (2 * LANES)) * LANES
         return (lanes[0], middle), (middle, lanes[1])
 
     def along_x(d, lanes):
@@ -205,41 +213,44 @@
                 for dx, part in zip(x_near, halves(lanes)):
                     unit = w_unit(-d, xrel(2), c, part)
                     links.recv(("x2", lanes, -d % Z, dx), unit, dev(dx=-dx))
-            theirs = w_bundle(xrel(2), c, lanes)
-            links.send(("wc", lanes, 2), theirs, theirs, dev(dc=1))
+                unit = w_unit(-d, xrel(2), c, lanes)
+                links.send(("wc2", lanes, d), unit, unit, dev(dc=1))
 
     def core_last(lanes):
-        for dx in range(X):
+        for dx in [0] + [dx % X for dx in x_near]:
             links.recv(("wc", lanes, dx), w_bundle(xrel(-dx), co, lanes), dev(dc=1))
-
-    for lanes in (KV, QF):
+        if X > 2:
+            for d in near_first:
+                links.recv(("wc2", lanes, d), w_unit(-d, xrel(2), co, lanes), dev(dc=1))
+
+    for lanes in (KVF, Q):
         for d in far_first:
             unit = w_unit(0, x, c, lanes)
             links.send(("wz", lanes, d), unit, unit, dev(dz=d))
     for dy in y_near:
         links.send(("tok", dy), t_rows(y), t_rows(y), dev(dy=dy))
     for d in far_first:
-        links.send(("woz", d), wo_ref, wo_block(c, x, z, y), dev(dz=d))
+        links.send(("woz", d), WO_OWN, wo_block(c, x, z, y), dev(dz=d))
 
     QB[...] = jnp.zeros_like(QB)
     VT[:, HEAD_DIM:, :] = jnp.ones((2, VT.shape[1] - HEAD_DIM, VT.shape[2]), jnp.bfloat16)
     M[...] = jnp.full(M.shape, LOW, jnp.float32)
     ACC[...] = jnp.zeros_like(ACC)
 
-    z_stage(KV)
+    z_stage(KVF)
     for dy, lo in zip(y_near, (0, TB // 2)):
         links.recv(("tok", dy), t_rows(yrel(-dy)), dev(dy=-dy))
         if Y > 2:
             part = t_rows(yrel(-dy), lo, TB // 2)
             links.send(("tok2", dy), part, part, dev(dy=dy))
-    x_stage(KV)
-    z_stage(QF)
-    x_last(KV)
-    x_stage(QF)
+    x_stage(KVF)
+    z_stage(Q)
+    x_last(KVF)
+    x_stage(Q)
     if Y > 2:
         for dy, lo in zip(y_near, (0, TB // 2)):
             links.recv(("tok2", dy), t_rows(yrel(2), lo, TB // 2), dev(dy=-dy))
-    core_last(KV)
+    core_last(KVF)
 
     rows = XN[...]
 
@@ -253,30 +264,10 @@
     def k_block(cc, zz, xx):
         return K.at[pl.ds(pl.multiple_of(slot(cc, zz, xx), LANES), HB), :]
 
-    def v_block(p, cc, zz, xx):
-        return VT.at[p, 0:HEAD_DIM, pl.ds(pl.multiple_of(slot(cc, zz, xx), LANES), HB)]
-
-    k_all = project(0, WC)
-    for h in range(X):
-        kh = k_all[:, h * HEAD_DIM : (h + 1) * HEAD_DIM]
-        KS[h] = jnp.concatenate([kh[:HB], kh[HB:]], axis=1).astype(jnp.bfloat16)
-    for dx in range(1, X):
-        links.send(("k", dx), KS.at[xrel(dx)], k_block(c, z, x), dev(dx=dx))
-    v_all = project(WC, WC).T
-    for h in range(X):
-        vh = v_all[h * HEAD_DIM : (h + 1) * HEAD_DIM].astype(jnp.bfloat16)
-        VS[h, 0] = vh[:, :HB]
-        VS[h, 1] = vh[:, HB:]
-    for dx in range(1, X):
-        for p in range(2):
-            links.send(("v", p, dx), VS.at[xrel(dx), p], v_block(p, c, z, x), dev(dx=dx))
-    k_block(c, z, x)[...] = KS[x]
-    for p in range(2):
-        v_block(p, c, z, x)[...] = VS[x, p]
-
-    x_last(QF)
-    core_last(QF)
-    gates = project(3 * WC, LANES).T[:8]
+    def v_block(cc, zz, xx):
+        return VT.at[:, 0:HEAD_DIM, pl.ds(pl.multiple_of(slot(cc, zz, xx), LANES), HB)]
+
+    gates = project(2 * WC, LANES).T[:8]
     head_row = lax.broadcasted_iota(jnp.int32, gates.shape, 0)
     offset = jnp.zeros_like(gates)
     for h in range(X):
@@ -284,59 +275,73 @@
     GS[...] = log_sigmoid(gates + offset + math.log(GB * Z * X * C))
     for dx in range(1, X):
         links.send(("g", dx), GS, GX.at[x], dev(dx=dx))
-    q_all = project(2 * WC, WC)
+    GX[x] = GS[...]
+    k_all = project(0, WC)
+    for h in range(X):
+        kh = k_all[:, h * HEAD_DIM : (h + 1) * HEAD_DIM]
+        KS[h] = jnp.concatenate([kh[:HB], kh[HB:]], axis=1).astype(jnp.bfloat16)
+    for dx in range(1, X):
+        links.send(("k", dx), KS.at[xrel(dx)], k_block(c, z, x), dev(dx=dx))
+    x_last(Q)
+    v_all = project(WC, WC).T
+    for h in range(X):
+        vh = v_all[h * HEAD_DIM : (h + 1) * HEAD_DIM].astype(jnp.bfloat16)
+        VS[h, 0] = vh[:, :HB]
+        VS[h, 1] = vh[:, HB:]
+    for dx in range(1, X):
+        links.send(("v", dx), VS.at[xrel(dx)], v_block(c, z, x), dev(dx=dx))
+    k_block(c, z, x)[...] = KS[x]
+    v_block(c, z, x)[...] = VS[x]
+
+    UP = DN = Z // 2
+
+    def goes(way, a, k):
+        return k < UP or (k == UP and (a == 0) == (way == "up"))
+
+    def bundle(zz, cc):
+        at = pl.multiple_of(slot(cc, zz, 0), LANES)
+        return K.at[pl.ds(at, X * HB), :], VT.at[:, 0:HEAD_DIM, pl.ds(at, X * HB)]
+
+    def piece(zz, dx):
+        return k_block(c, zz, xrel(-dx)), v_block(c, zz, xrel(-dx))
+
+    WAYS = (("up", 1), ("dn", -1))
+    pieces = [0] + ([1, X - 1] if X > 2 else [1]) + list(range(2, X - 1))
+
+    def ring_start(dx):
+        for a, view in enumerate(piece(z, dx)):
+            for way, sign in WAYS:
+                if goes(way, a, 1):
+                    links.send((way, 1, dx, a), view, view, dev(dz=sign))
+
+    def to_core(d):
+        for a, view in enumerate(bundle(zrel(d), c)):
+            links.send(("core", d % Z, a), view, view, dev(dc=1))
+
+    def ring_step(k, some):
+        for dx in some:
+            for a in range(2):
+                for way, sign in WAYS:
+                    if goes(way, a, k):
+                        view = piece(zrel(-sign * k), dx)[a]
+                        links.recv((way, k, dx, a), view, dev(dz=-sign))
+                        if goes(way, a, k + 1):
+                            links.send((way, k + 1, dx, a), view, view, dev(dz=sign))
+
+    def other_core(d):
+        for a, view in enumerate(bundle(zrel(d), co)):
+            links.recv(("core", d % Z, a), view, dev(dc=1))
+
+    ring_start(0)
+    core_last(Q)
+    q_all = project(KVF[1], WC)
     q_all = q_all.astype(jnp.bfloat16).astype(jnp.float32) * (HEAD_DIM**-0.5 * LOG2E)
     q_all = q_all.T
     for h in range(X):
         QS[h] = q_all[h * HEAD_DIM : (h + 1) * HEAD_DIM].astype(jnp.bfloat16)
     for dx in range(1, X):
         links.send(("q", dx), QS.at[xrel(dx)], QT.at[x], dev(dx=dx))
-    GX[x] = GS[...]
     QT[x] = QS[x]
-
-    UP = DN = Z // 2
-
-    def goes(way, a, k):
-        return k < UP or (k == UP and (a == 0) == (way == "up"))
-
-    def kv(zz, cc):
-        at = pl.multiple_of(slot(cc, zz, 0), LANES)
-        return [
-            K.at[pl.ds(at, X * HB), :],
-            VT.at[0, 0:HEAD_DIM, pl.ds(at, X * HB)],
-            VT.at[1, 0:HEAD_DIM, pl.ds(at, X * HB)],
-        ]
-
-    WAYS = (("up", 1), ("dn", -1))
-
-    def ring_start():
-        for a, view in enumerate(kv(z, c)):
-            for way, sign in WAYS:
-                if goes(way, a, 1):
-                    links.send((way, 1, a), view, view, dev(dz=sign))
-        for a, view in enumerate(kv(z, c)):
-            links.send(("core", 0, a), view, view, dev(dc=1))
-
-    def ring_step(k):
-        for a in range(3):
-            for way, sign in WAYS:
-                if goes(way, a, k):
-                    view = kv(zrel(-sign * k), c)[a]
-                    links.recv((way, k, a), view, dev(dz=-sign))
-                    if goes(way, a, k + 1):
-                        links.send((way, k + 1, a), view, view, dev(dz=sign))
-                    links.send(("core", -sign * k % Z, a), view, view, dev(dc=1))
-
-    def other_core(d):
-        for a, view in enumerate(kv(zrel(d), co)):
-            links.recv(("core", d % Z, a), view, dev(dc=1))
-
-    for dx in range(1, X):
-        sx = xrel(-dx)
-        links.recv(("k", dx), k_block(c, z, sx), dev(dx=-dx))
-        for p in range(2):
-            links.recv(("v", p, dx), v_block(p, c, z, sx), dev(dx=-dx))
-    ring_start()
 
     for dx in range(1, X):
         links.recv(("g", dx), GX.at[xrel(-dx)], dev(dx=-dx))
@@ -357,6 +362,13 @@
     G[z] = chip_gates
     for d in far_first:
         links.send(("gz", d), G.at[z], G.at[z], dev(dz=d))
+    for dx in pieces[1:]:
+        sx = xrel(-dx)
+        links.recv(("k", dx), k_block(c, z, sx), dev(dx=-dx))
+        links.recv(("v", dx), v_block(c, z, sx), dev(dx=-dx))
+        ring_start(dx)
+    to_core(0)
+
     for dx in range(1, X):
         links.recv(("q", dx), QT.at[xrel(-dx)], dev(dx=-dx))
     for sx in range(X):
@@ -453,14 +465,7 @@
     cum_here = cumulative(G[z])
     cum_q_here = query_sums(cum_here)
 
-    @pl.loop(0, 2)
-    def _(i):
-        cc = jnp.where(i == 0, c, co)
-
-        @pl.when(i == 1)
-        def _():
-            other_core(0)
-
+    def present(cc):
         def masked(pair):
             def mask(s, which, t):
                 r = lax.broadcasted_iota(jnp.int32, s.shape, 0)
@@ -479,35 +484,15 @@
         ]
         attend(items, cum_q_here)
 
-    for d in far_first:
-        links.recv(("gz", d), G.at[zrel(-d)], dev(dz=-d))
-    CUM[...] = cumulative(G[...].reshape(Z * 8, GB)).reshape(Z, 8, GB)
-    cum_q = query_sums(CUM[z])
-
-    def past(ds):
-        @pl.loop(0, 2)
-        def _(i):
-            cc = jnp.where(i == 0, c, co)
-
-            @pl.when(i == 1)
-            def _():
-                for d in ds:
-                    other_core(d)
-
-            items = []
-            for d in ds:
-                zz = zrel(d)
-                table = key_sums(CUM[zz], cc)
-                items += [
-                    (table, slot(cc, zz, 0), pair, t, None)
-                    for pair in range(X // 2)
-                    for t in range(X)
-                ]
-            attend(items, cum_q)
-
-    def skipped(ds):
+    def past(ds, cc):
+        items = []
         for d in ds:
-            other_core(d)
+            zz = zrel(d)
+            table = key_sums(CUM[zz], cc)
+            items += [
+                (table, slot(cc, zz, 0), pair, t, None) for pair in range(X // 2) for t in range(X)
+            ]
+        attend(items, query_sums(CUM[z]))
 
     def wo_forward():
         for dx, dy in plane:
@@ -515,40 +500,59 @@
             links.recv(("woxy", dx, dy), theirs, dev(dx=-dx, dy=-dy))
             links.send(("woc", dx, dy), theirs, theirs, dev(dc=1))
 
+    def step_back(k, cc):
+        if k == 0:
+            present(cc)
+        elif k < UP:
+
+            @pl.when(z + k >= Z)
+            def _():
+                past([-k, k], cc)
+
+            @pl.when((z >= k) & (z + k < Z))
+            def _():
+                past([-k], cc)
+
+        else:
+
+            @pl.when(z >= k)
+            def _():
+                past([-k], cc)
+
+    def came(k):
+        for d in [-k, k] if 0 < k < UP else [-k]:
+            other_core(d)
+
+    cut = (len(pieces) + 1) // 2
     for k in range(1, UP + 1):
-        ring_step(k)
+        ring_step(k, pieces[:cut])
+        step_back(k - 1, c)
+        ring_step(k, pieces[cut:])
+        to_core(-k)
+        if k < UP:
+            to_core(k)
         if k == UP:
             wo_forward()
-        both = [-k, k] if k < UP else [-k]
-        if k < UP:
-
-            @pl.when(z + k >= Z)
-            def _():
-                past(both)
-
-            @pl.when((z >= k) & (z + k < Z))
-            def _():
-                past([-k])
-                skipped([k])
-
-        else:
-
-            @pl.when(z >= k)
-            def _():
-                past(both)
-
-        @pl.when(z < k)
-        def _():
-            skipped(both)
+        came(k - 1)
+        step_back(k - 1, co)
+        if k == 1:
+            for d in far_first:
+                links.recv(("gz", d), G.at[zrel(-d)], dev(dz=-d))
+            CUM[...] = cumulative(G[...].reshape(Z * 8, GB)).reshape(Z, 8, GB)
+    step_back(UP, c)
+    came(UP)
+    step_back(UP, co)
 
     for t in range(X):
         acc = ACC[t]
         o = (acc[:HEAD_DIM] / acc[HEAD_DIM : HEAD_DIM + 1]).astype(jnp.bfloat16)
         for yy in range(Y):
-            OS[t, yy, :, 0:TB] = o[:, yy * TB : (yy + 1) * TB]
+            part = o[:, yy * TB : (yy + 1) * TB]
+            for h in range(2):
+                OS[t, yy, :, h * TB : (h + 1) * TB] = part[h * HALF : (h + 1) * HALF]
 
     def at_rows(xx, yy):
-        return AT.at[pl.ds(pl.multiple_of((yy * X + xx) * HEAD_DIM, HEAD_DIM), HEAD_DIM), :]
+        return AT.at[pl.ds(pl.multiple_of((yy * X + xx) * HALF, HALF), HALF), :]
 
     for dx, dy in plane:
         links.send(("o", dx, dy), OS.at[xrel(dx), yrel(dy)], at_rows(x, y), dev(dx=dx, dy=dy))
@@ -564,12 +568,15 @@
     for cc in range(C):
         for xx in range(X):
             block = (cc * X + xx) * Z * PR
-            part = jnp.dot(
-                WO[block : block + Z * PR, :], attended, preferred_element_type=jnp.float32
+            part = sum(
+                jnp.dot(WO[h, block : block + Z * PR, :], attended, preferred_element_type=jnp.float32)[
+                    :, h * TB : (h + 1) * TB
+                ]
+                for h in range(2)
             )
             for zz in range(Z):
                 to = ((zz * X + xx) * C + cc) * PR
-                PT[to : to + PR, :] = part[zz * PR : (zz + 1) * PR]
+                PT[to : to + PR, 0:TB] = part[zz * PR : (zz + 1) * PR]
     out_ref[...] = rms_norm(PT[...].T[:TB], ogain_ref[...])
     links.drain()
 
@@ -582,13 +589,13 @@
     HB = GB // 2
     LW = 3 * WC + LANES
     keys = Z * X * C * HB
-    n_sems = 260
+    n_sems = 340
     vmem, smem = pl.BlockSpec(memory_space=pltpu.VMEM), pl.BlockSpec(memory_space=pltpu.SMEM)
     bf16, f32 = jnp.bfloat16, jnp.float32
     scratch = [
         pltpu.VMEM((Z, X * C * PR, LW), bf16),
         pltpu.VMEM((GB, D), bf16),
-        pltpu.VMEM((D, D), bf16),
+        pltpu.VMEM((2, D, D // 2), bf16),
         pltpu.VMEM((X, HB, LANES), bf16),
         pltpu.VMEM((X, 2, HEAD_DIM, HB), bf16),
         pltpu.VMEM((X, HEAD_DIM, GB), bf16),
@@ -604,11 +611,12 @@
         pltpu.VMEM((X, LANES, 2 * GB), bf16),
         pltpu.VMEM((X, 1, GB), f32),
         pltpu.VMEM((X, HEAD_DIM + 16, GB), f32),
-        pltpu.VMEM((X, Y, HEAD_DIM, LANES), bf16),
-        pltpu.VMEM((D, LANES), bf16),
+        pltpu.VMEM((X, Y, HEAD_DIM // 2, 2 * TB), bf16),
+        pltpu.VMEM((D // 2, 2 * TB), bf16),
         pltpu.VMEM((D, LANES), f32),
         pltpu.VMEM((3, 2, 2 * HB, GB), f32),
         pltpu.VMEM((2, 4 * HB, GB), bf16),
+        pltpu.VMEM((2, PR, WC // 2), bf16),
         pltpu.SemaphoreType.DMA((n_sems,)),
         pltpu.SemaphoreType.DMA((n_sems,)),
     ]
@@ -627,7 +635,7 @@
         w_query,
         w_key,
         w_value,
-        w_forget,
+        w_forget.T,
         forget_offset,
         w_out_t,
         out_gain.reshape(1, D),

time: 79.3 us -> 74 us (0.933)
  the two profiles are of different devices: /device:TPU:1 before, /device:TPU:224 now
where the time goes in v3:
time: 74 us; the launch traced here: 73.9 us
  Pallas kernels  72.3 us (98%)
  local copies, waits for them, and re-layouts  1.57 us (2%)
    pallas_call x1, Pallas kernels, layer(): pl.pallas_call(functools.partial(kernel, dims), out_shape=jax.ShapeDtypeS...  72.3 us
    unnamed x1, local copies, waits for them, and re-layouts  1.57 us

profile of v3, /device:TPU:224, one launch (start us, length us, event | category | flops | bytes accessed | tf_op | source)
XLA Modules:
  0.0 73.9 jit_solution(9909115198402339295)
XLA Ops:
  0.0 72.3 %shard_map.91 = bf16[64,1024]{1,0:T(8,128)(2,1)} custom-call(bf16[64,1024]{1,0:T(8,128)(2,1)} %tokens_ref.1, f32[1,1024]{1,0:T(1,128)} %bitcast.3, bf16[16,256]{1,0:T(8,128)(2,1)} %wq_ref.1, bf16[16,256]{1,0:T(8,128)(2,1)} %wk_ref.1, bf16[16,256]{1,0:T(8,128)(2,1)} %wv_ref.1, bf16[4,16]{1,0:T(4,128)(2,1)} %bitcast.5, f32[4]{0:T(128)} %off_ref.1, ...), custom_call_target="tpu_custom_call" | custom-call | tf_op jit(solution)/shard_map/pallas_call | solution.py:623
  72.3 1.6 %copy.11 = bf16[64,1024]{1,0:T(8,128)(2,1)} copy(bf16[64,1024]{1,0:T(8,128)(2,1)} %shard_map.91) | data formatting | bytes 262144

commit v4 on v3

--- a/solution.py
+++ b/solution.py
@@ -30,31 +30,42 @@
 
 
 class Links:
-    def __init__(self, send_sems, recv_sems, ids):
-        self.send_sems, self.recv_sems, self.ids, self.sent = send_sems, recv_sems, ids, []
+    def __init__(self, send_sems, recv_sems, counter):
+        self.send_sems, self.recv_sems, self.counter = send_sems, recv_sems, counter
+        self.ids, self.sent = {}, [0]
+        self.most = counter.shape[0]
 
     def copy(self, key, src, dst, dev):
-        at = self.ids.setdefault(key, len(self.ids))
         return pltpu.make_async_remote_copy(
             src_ref=src,
             dst_ref=dst,
-            send_sem=self.send_sems.at[at],
-            recv_sem=self.recv_sems.at[at],
+            send_sem=self.send_sems.at[len(self.sent) - 1],
+            recv_sem=self.recv_sems.at[self.ids.setdefault(key, len(self.ids))],
             device_id=dev,
             device_id_type=MESH,
         )
 
     def send(self, key, src, dst, dev):
-        c = self.copy(key, src, dst, dev)
-        c.start()
-        self.sent.append(c)
+        rows = math.prod(src.shape) * src.dtype.itemsize // (2 * LANES)
+        if self.sent[-1] + rows > self.most:
+            self.sent.append(0)
+        self.sent[-1] += rows
+        self.copy(key, src, dst, dev).start()
 
     def recv(self, key, landed, dev):
         self.copy(key, landed, landed, dev).wait_recv()
 
-    def drain(self):
-        for c in self.sent:
-            c.wait_send()
+    def drain(self, dev):
+        for at, rows in enumerate(self.sent):
+            view = self.counter.at[0:rows]
+            pltpu.make_async_remote_copy(
+                src_ref=view,
+                dst_ref=view,
+                send_sem=self.send_sems.at[at],
+                recv_sem=self.recv_sems.at[0],
+                device_id=dev,
+                device_id_type=MESH,
+            ).wait_send()
 
 
 def kernel(
@@ -103,7 +114,7 @@
     PR, WC = wo_ref.shape
     LW = W.shape[2]
     z, x, c, y = (lax.axis_index(a) for a in AXES)
-    links = Links(send_sems, recv_sems, {})
+    links = Links(send_sems, recv_sems, K)
 
     def dev(dz=0, dx=0, dc=0, dy=0):
         return {
@@ -183,70 +194,77 @@
         middle = lanes[0] + -(-(lanes[1] - lanes[0]) // (2 * LANES)) * LANES
         return (lanes[0], middle), (middle, lanes[1])
 
-    def along_x(d, lanes):
+    opposite = X > 2
+
+    def fine_z(i, d):
+        if d != 0:
+            links.recv(("wz", d), w_unit(-d, x, c, KVF), dev(dz=-d))
         for dx in x_near:
-            unit = w_unit(d, x, c, lanes)
-            links.send(("x1", lanes, d, dx), unit, unit, dev(dx=dx))
-
-    def z_stage(lanes):
-        for d in near_first:
-            if d != 0:
-                links.recv(("wz", lanes, d), w_unit(-d, x, c, lanes), dev(dz=-d))
-            along_x(-d % Z, lanes)
-        own = w_bundle(x, c, lanes)
-        links.send(("wc", lanes, 0), own, own, dev(dc=1))
-
-    def x_stage(lanes):
-        for d in near_first:
-            for dx, part in zip(x_near, halves(lanes)):
-                links.recv(("x1", lanes, -d % Z, dx), w_unit(-d, xrel(-dx), c, lanes), dev(dx=-dx))
-                if X > 2:
-                    unit = w_unit(-d, xrel(-dx), c, part)
-                    links.send(("x2", lanes, -d % Z, dx), unit, unit, dev(dx=dx))
-        for dx in x_near:
-            theirs = w_bundle(xrel(-dx), c, lanes)
-            links.send(("wc", lanes, dx % X), theirs, theirs, dev(dc=1))
-
-    def x_last(lanes):
-        if X > 2:
-            for d in near_first:
-                for dx, part in zip(x_near, halves(lanes)):
-                    unit = w_unit(-d, xrel(2), c, part)
-                    links.recv(("x2", lanes, -d % Z, dx), unit, dev(dx=-dx))
-                unit = w_unit(-d, xrel(2), c, lanes)
-                links.send(("wc2", lanes, d), unit, unit, dev(dc=1))
+            unit = w_unit(-d, x, c, KVF)
+            links.send(("x1", d, dx), unit, unit, dev(dx=dx))
+
+    def fine_x(d):
+        for dx, part in zip(x_near, halves(KVF)):
+            links.recv(("x1", d, dx), w_unit(-d, xrel(-dx), c, KVF), dev(dx=-dx))
+            if opposite:
+                unit = w_unit(-d, xrel(-dx), c, part)
+                links.send(("x2", d, dx), unit, unit, dev(dx=dx))
+
+    def fine_last(d):
+        for dx, part in zip(x_near, halves(KVF)):
+            links.recv(("x2", d, dx), w_unit(-d, xrel(2), c, part), dev(dx=-dx))
+        unit = w_unit(-d, xrel(2), c, KVF)
+        links.send(("wc", KVF), unit, unit, dev(dc=1))
+
+    def to_other_core(xx, lanes):
+        view = w_bundle(xx, c, lanes)
+        links.send(("wc", lanes), view, view, dev(dc=1))
 
     def core_last(lanes):
-        for dx in [0] + [dx % X for dx in x_near]:
-            links.recv(("wc", lanes, dx), w_bundle(xrel(-dx), co, lanes), dev(dc=1))
-        if X > 2:
-            for d in near_first:
-                links.recv(("wc2", lanes, d), w_unit(-d, xrel(2), co, lanes), dev(dc=1))
+        links.recv(("wc", lanes), W.at[:, 0 : X * PR, lanes[0] : lanes[1]], dev(dc=1))
 
     for lanes in (KVF, Q):
         for d in far_first:
             unit = w_unit(0, x, c, lanes)
-            links.send(("wz", lanes, d), unit, unit, dev(dz=d))
+            links.send(("wz", d if lanes == KVF else Q), unit, unit, dev(dz=d))
     for dy in y_near:
         links.send(("tok", dy), t_rows(y), t_rows(y), dev(dy=dy))
     for d in far_first:
-        links.send(("woz", d), WO_OWN, wo_block(c, x, z, y), dev(dz=d))
+        links.send(("woz",), WO_OWN, wo_block(c, x, z, y), dev(dz=d))
 
     QB[...] = jnp.zeros_like(QB)
     VT[:, HEAD_DIM:, :] = jnp.ones((2, VT.shape[1] - HEAD_DIM, VT.shape[2]), jnp.bfloat16)
     M[...] = jnp.full(M.shape, LOW, jnp.float32)
     ACC[...] = jnp.zeros_like(ACC)
 
-    z_stage(KVF)
-    for dy, lo in zip(y_near, (0, TB // 2)):
-        links.recv(("tok", dy), t_rows(yrel(-dy)), dev(dy=-dy))
-        if Y > 2:
-            part = t_rows(yrel(-dy), lo, TB // 2)
-            links.send(("tok2", dy), part, part, dev(dy=dy))
-    x_stage(KVF)
-    z_stage(Q)
-    x_last(KVF)
-    x_stage(Q)
+    LAG = 3
+    for i in range(Z + LAG):
+        if i < Z:
+            fine_z(i, near_first[i])
+        if i >= LAG:
+            fine_x(near_first[i - LAG])
+        if i == min(5, Z):
+            for dy, lo in zip(y_near, (0, TB // 2)):
+                links.recv(("tok", dy), t_rows(yrel(-dy)), dev(dy=-dy))
+                if Y > 2:
+                    part = t_rows(yrel(-dy), lo, TB // 2)
+                    links.send(("tok2", dy), part, part, dev(dy=dy))
+    for dx in [0] + x_near:
+        to_other_core(xrel(-dx), KVF)
+    links.recv(("wz", Q), W.at[0 : Z - 1, 0:PR, Q[0] : Q[1]], dev(dz=1))
+    for dx in x_near:
+        view = w_bundle(x, c, Q)
+        links.send(("x1", Q, dx), view, view, dev(dx=dx))
+    if opposite:
+        for d in near_first:
+            fine_last(d)
+    for dx, part in zip(x_near, halves(Q)):
+        links.recv(("x1", Q, dx), w_bundle(xrel(-dx), c, Q), dev(dx=-dx))
+        if opposite:
+            view = w_bundle(xrel(-dx), c, part)
+            links.send(("x2", Q, dx), view, view, dev(dx=dx))
+    for dx in [0] + x_near:
+        to_other_core(xrel(-dx), Q)
     if Y > 2:
         for dy, lo in zip(y_near, (0, TB // 2)):
             links.recv(("tok2", dy), t_rows(yrel(2), lo, TB // 2), dev(dy=-dy))
@@ -274,22 +292,25 @@
         offset = jnp.where(head_row == h, off_ref[h], offset)
     GS[...] = log_sigmoid(gates + offset + math.log(GB * Z * X * C))
     for dx in range(1, X):
-        links.send(("g", dx), GS, GX.at[x], dev(dx=dx))
+        links.send(("g",), GS, GX.at[x], dev(dx=dx))
     GX[x] = GS[...]
     k_all = project(0, WC)
     for h in range(X):
         kh = k_all[:, h * HEAD_DIM : (h + 1) * HEAD_DIM]
         KS[h] = jnp.concatenate([kh[:HB], kh[HB:]], axis=1).astype(jnp.bfloat16)
     for dx in range(1, X):
-        links.send(("k", dx), KS.at[xrel(dx)], k_block(c, z, x), dev(dx=dx))
-    x_last(Q)
+        links.send(("kv", dx), KS.at[xrel(dx)], k_block(c, z, x), dev(dx=dx))
+    if opposite:
+        for dx, part in zip(x_near, halves(Q)):
+            links.recv(("x2", Q, dx), w_bundle(xrel(2), c, part), dev(dx=-dx))
+        to_other_core(xrel(2), Q)
     v_all = project(WC, WC).T
     for h in range(X):
         vh = v_all[h * HEAD_DIM : (h + 1) * HEAD_DIM].astype(jnp.bfloat16)
         VS[h, 0] = vh[:, :HB]
         VS[h, 1] = vh[:, HB:]
     for dx in range(1, X):
-        links.send(("v", dx), VS.at[xrel(dx)], v_block(c, z, x), dev(dx=dx))
+        links.send(("kv", dx), VS.at[xrel(dx)], v_block(c, z, x), dev(dx=dx))
     k_block(c, z, x)[...] = KS[x]
     v_block(c, z, x)[...] = VS[x]
 
@@ -312,25 +333,24 @@
         for a, view in enumerate(piece(z, dx)):
             for way, sign in WAYS:
                 if goes(way, a, 1):
-                    links.send((way, 1, dx, a), view, view, dev(dz=sign))
+                    links.send((way, 1, dx), view, view, dev(dz=sign))
 
     def to_core(d):
-        for a, view in enumerate(bundle(zrel(d), c)):
-            links.send(("core", d % Z, a), view, view, dev(dc=1))
+        for view in bundle(zrel(d), c):
+            links.send(("core", d % Z), view, view, dev(dc=1))
 
     def ring_step(k, some):
         for dx in some:
-            for a in range(2):
-                for way, sign in WAYS:
-                    if goes(way, a, k):
+            for way, sign in WAYS:
+                arrays = [a for a in range(2) if goes(way, a, k)]
+                links.recv((way, k, dx), K.at[0 : len(arrays) * HB], dev(dz=-sign))
+                for a in arrays:
+                    if goes(way, a, k + 1):
                         view = piece(zrel(-sign * k), dx)[a]
-                        links.recv((way, k, dx, a), view, dev(dz=-sign))
-                        if goes(way, a, k + 1):
-                            links.send((way, k + 1, dx, a), view, view, dev(dz=sign))
+                        links.send((way, k + 1, dx), view, view, dev(dz=sign))
 
     def other_core(d):
-        for a, view in enumerate(bundle(zrel(d), co)):
-            links.recv(("core", d % Z, a), view, dev(dc=1))
+        links.recv(("core", d % Z), K.at[0 : 2 * X * HB], dev(dc=1))
 
     ring_start(0)
     core_last(Q)
@@ -340,11 +360,10 @@
     for h in range(X):
         QS[h] = q_all[h * HEAD_DIM : (h + 1) * HEAD_DIM].astype(jnp.bfloat16)
     for dx in range(1, X):
-        links.send(("q", dx), QS.at[xrel(dx)], QT.at[x], dev(dx=dx))
+        links.send(("q",), QS.at[xrel(dx)], QT.at[x], dev(dx=dx))
     QT[x] = QS[x]
 
-    for dx in range(1, X):
-        links.recv(("g", dx), GX.at[xrel(-dx)], dev(dx=-dx))
+    links.recv(("g",), GX.at[0 : X - 1], dev(dx=1))
     row8 = lax.broadcasted_iota(jnp.int32, (8, GB), 0)
     own_gates = jnp.zeros((8, GB), jnp.float32)
     for sx in range(X):
@@ -361,25 +380,21 @@
         chip_gates = jnp.where(row8 == 2 * sx + 1, jnp.where(c == 0, b, a), chip_gates)
     G[z] = chip_gates
     for d in far_first:
-        links.send(("gz", d), G.at[z], G.at[z], dev(dz=d))
+        links.send(("gz",), G.at[z], G.at[z], dev(dz=d))
     for dx in pieces[1:]:
-        sx = xrel(-dx)
-        links.recv(("k", dx), k_block(c, z, sx), dev(dx=-dx))
-        links.recv(("v", dx), v_block(c, z, sx), dev(dx=-dx))
+        links.recv(("kv", dx), K.at[0 : 2 * HB], dev(dx=-dx))
         ring_start(dx)
     to_core(0)
 
-    for dx in range(1, X):
-        links.recv(("q", dx), QT.at[xrel(-dx)], dev(dx=-dx))
+    links.recv(("q",), QT.at[0 : X - 1], dev(dx=1))
     for sx in range(X):
         QB[sx, 0:HEAD_DIM, 0:GB] = QT[sx]
         QB[sx, HEAD_DIM:, GB:] = QT[sx]
-    for d in far_first:
-        links.recv(("woz", d), wo_block(c, x, zrel(-d), y), dev(dz=-d))
+    links.recv(("woz",), WO.at[:, 0 : (Z - 1) * PR, 0:WH], dev(dz=1))
     own = wo_bundle(c, x, y)
     for dx, dy in plane:
-        links.send(("woxy", dx, dy), own, own, dev(dx=dx, dy=dy))
-    links.send(("woc", 0, 0), own, own, dev(dc=1))
+        links.send(("woxy",), own, own, dev(dx=dx, dy=dy))
+    links.send(("woc",), own, own, dev(dc=1))
 
     def cumulative(block):
         n = block.shape[0]
@@ -494,11 +509,14 @@
             ]
         attend(items, query_sums(CUM[z]))
 
+    def wo_rows(bundles):
+        return bundles * Z * PR * WH // WO.shape[2]
+
     def wo_forward():
+        links.recv(("woxy",), WO.at[:, 0 : wo_rows(len(plane)), :], dev(dx=1))
         for dx, dy in plane:
             theirs = wo_bundle(c, xrel(-dx), yrel(-dy))
-            links.recv(("woxy", dx, dy), theirs, dev(dx=-dx, dy=-dy))
-            links.send(("woc", dx, dy), theirs, theirs, dev(dc=1))
+            links.send(("woc",), theirs, theirs, dev(dc=1))
 
     def step_back(k, cc):
         if k == 0:
@@ -536,8 +554,7 @@
         came(k - 1)
         step_back(k - 1, co)
         if k == 1:
-            for d in far_first:
-                links.recv(("gz", d), G.at[zrel(-d)], dev(dz=-d))
+            links.recv(("gz",), G.at[0 : Z - 1], dev(dz=1))
             CUM[...] = cumulative(G[...].reshape(Z * 8, GB)).reshape(Z, 8, GB)
     step_back(UP, c)
     came(UP)
@@ -555,14 +572,10 @@
         return AT.at[pl.ds(pl.multiple_of((yy * X + xx) * HALF, HALF), HALF), :]
 
     for dx, dy in plane:
-        links.send(("o", dx, dy), OS.at[xrel(dx), yrel(dy)], at_rows(x, y), dev(dx=dx, dy=dy))
+        links.send(("o",), OS.at[xrel(dx), yrel(dy)], at_rows(x, y), dev(dx=dx, dy=dy))
     at_rows(x, y)[...] = OS[x, y]
-    for dx in range(X):
-        for dy in range(Y):
-            theirs = wo_bundle(co, xrel(-dx), yrel(-dy))
-            links.recv(("woc", dx, dy), theirs, dev(dc=1))
-    for dx, dy in plane:
-        links.recv(("o", dx, dy), at_rows(xrel(-dx), yrel(-dy)), dev(dx=-dx, dy=-dy))
+    links.recv(("woc",), WO.at[:, 0 : wo_rows(X * Y), :], dev(dc=1))
+    links.recv(("o",), AT.at[0 : len(plane) * HALF], dev(dx=1))
 
     attended = AT[...]
     for cc in range(C):
@@ -578,7 +591,7 @@
                 to = ((zz * X + xx) * C + cc) * PR
                 PT[to : to + PR, 0:TB] = part[zz * PR : (zz + 1) * PR]
     out_ref[...] = rms_norm(PT[...].T[:TB], ogain_ref[...])
-    links.drain()
+    links.drain(dev(dc=1))
 
 
 def layer(dims, tokens, norm_gain, w_query, w_key, w_value, w_forget, forget_offset, w_out_t, out_gain):
@@ -589,7 +602,7 @@
     HB = GB // 2
     LW = 3 * WC + LANES
     keys = Z * X * C * HB
-    n_sems = 340
+    n_sems = 101
     vmem, smem = pl.BlockSpec(memory_space=pltpu.VMEM), pl.BlockSpec(memory_space=pltpu.SMEM)
     bf16, f32 = jnp.bfloat16, jnp.float32
     scratch = [
@@ -617,7 +630,7 @@
         pltpu.VMEM((3, 2, 2 * HB, GB), f32),
         pltpu.VMEM((2, 4 * HB, GB), bf16),
         pltpu.VMEM((2, PR, WC // 2), bf16),
-        pltpu.SemaphoreType.DMA((n_sems,)),
+        pltpu.SemaphoreType.DMA((5,)),
         pltpu.SemaphoreType.DMA((n_sems,)),
     ]
     return pl.pallas_call(

time: 74 us -> 71.8 us (0.970)
  Pallas kernels: 72.3 us -> 70.1 us
    pallas_call x1, Pallas kernels: 72.3 us -> 70.1 us  [layer(): pl.pallas_call(functools.partial(kernel, dims), out_shape=jax.ShapeDtypeS...]
where the time goes in v4:
time: 71.8 us; the launch traced here: 71.7 us
  Pallas kernels  70.1 us (98%)
  local copies, waits for them, and re-layouts  1.57 us (2%)
    pallas_call x1, Pallas kernels, layer(): pl.pallas_call(functools.partial(kernel, dims), out_shape=jax.ShapeDtypeS...  70.1 us
    unnamed x1, local copies, waits for them, and re-layouts  1.57 us

profile of v4, /device:TPU:224, one launch (start us, length us, event | category | flops | bytes accessed | tf_op | source)
XLA Modules:
  0.0 71.7 jit_solution(16380666509116044429)
XLA Ops:
  0.0 70.1 %shard_map.91 = bf16[64,1024]{1,0:T(8,128)(2,1)} custom-call(bf16[64,1024]{1,0:T(8,128)(2,1)} %tokens_ref.1, f32[1,1024]{1,0:T(1,128)} %bitcast.3, bf16[16,256]{1,0:T(8,128)(2,1)} %wq_ref.1, bf16[16,256]{1,0:T(8,128)(2,1)} %wk_ref.1, bf16[16,256]{1,0:T(8,128)(2,1)} %wv_ref.1, bf16[4,16]{1,0:T(4,128)(2,1)} %bitcast.5, f32[4]{0:T(128)} %off_ref.1, ...), custom_call_target="tpu_custom_call" | custom-call | tf_op jit(solution)/shard_map/pallas_call | solution.py:636
  70.1 1.6 %copy.11 = bf16[64,1024]{1,0:T(8,128)(2,1)} copy(bf16[64,1024]{1,0:T(8,128)(2,1)} %shard_map.91) | data formatting | bytes 262144

commit v5 on v4

--- a/solution.py
+++ b/solution.py
@@ -196,7 +196,7 @@
 
     opposite = X > 2
 
-    def fine_z(i, d):
+    def fine_z(d):
         if d != 0:
             links.recv(("wz", d), w_unit(-d, x, c, KVF), dev(dz=-d))
         for dx in x_near:
@@ -237,19 +237,17 @@
     M[...] = jnp.full(M.shape, LOW, jnp.float32)
     ACC[...] = jnp.zeros_like(ACC)
 
-    LAG = 3
-    for i in range(Z + LAG):
-        if i < Z:
-            fine_z(i, near_first[i])
-        if i >= LAG:
-            fine_x(near_first[i - LAG])
-        if i == min(5, Z):
-            for dy, lo in zip(y_near, (0, TB // 2)):
-                links.recv(("tok", dy), t_rows(yrel(-dy)), dev(dy=-dy))
-                if Y > 2:
-                    part = t_rows(yrel(-dy), lo, TB // 2)
-                    links.send(("tok2", dy), part, part, dev(dy=dy))
-    for dx in [0] + x_near:
+    for d in near_first:
+        fine_z(d)
+    to_other_core(x, KVF)
+    for dy, lo in zip(y_near, (0, TB // 2)):
+        links.recv(("tok", dy), t_rows(yrel(-dy)), dev(dy=-dy))
+        if Y > 2:
+            part = t_rows(yrel(-dy), lo, TB // 2)
+            links.send(("tok2", dy), part, part, dev(dy=dy))
+    for d in near_first:
+        fine_x(d)
+    for dx in x_near:
         to_other_core(xrel(-dx), KVF)
     links.recv(("wz", Q), W.at[0 : Z - 1, 0:PR, Q[0] : Q[1]], dev(dz=1))
     for dx in x_near:
@@ -371,6 +369,12 @@
         own_gates = jnp.where(row8 == sx, picked, own_gates)
     GP[...] = own_gates
     links.send(("gp",), GP, GPR, dev(dc=1))
+    def next_piece(dx):
+        links.recv(("kv", dx), K.at[0 : 2 * HB], dev(dx=-dx))
+        ring_start(dx)
+
+    for dx in pieces[1:-1]:
+        next_piece(dx)
     links.recv(("gp",), GPR, dev(dc=1))
     theirs = GPR[...]
     chip_gates = jnp.zeros((8, GB), jnp.float32)
@@ -381,9 +385,8 @@
     G[z] = chip_gates
     for d in far_first:
         links.send(("gz",), G.at[z], G.at[z], dev(dz=d))
-    for dx in pieces[1:]:
-        links.recv(("kv", dx), K.at[0 : 2 * HB], dev(dx=-dx))
-        ring_start(dx)
+    for dx in pieces[-1:]:
+        next_piece(dx)
     to_core(0)
 
     links.recv(("q",), QT.at[0 : X - 1], dev(dx=1))

time: 71.8 us -> 69 us (0.961)
  Pallas kernels: 70.1 us -> 67.3 us
    pallas_call x1, Pallas kernels: 70.1 us -> 67.3 us  [layer(): pl.pallas_call(functools.partial(kernel, dims), out_shape=jax.ShapeDtypeS...]
where the time goes in v5:
time: 69 us; the launch traced here: 68.9 us
  Pallas kernels  67.3 us (98%)
  local copies, waits for them, and re-layouts  1.57 us (2%)
    pallas_call x1, Pallas kernels, layer(): pl.pallas_call(functools.partial(kernel, dims), out_shape=jax.ShapeDtypeS...  67.3 us
    unnamed x1, local copies, waits for them, and re-layouts  1.57 us

profile of v5, /device:TPU:224, one launch (start us, length us, event | category | flops | bytes accessed | tf_op | source)
XLA Modules:
  0.0 68.9 jit_solution(10463656961560486775)
XLA Ops:
  0.0 67.3 %shard_map.91 = bf16[64,1024]{1,0:T(8,128)(2,1)} custom-call(bf16[64,1024]{1,0:T(8,128)(2,1)} %tokens_ref.1, f32[1,1024]{1,0:T(1,128)} %bitcast.3, bf16[16,256]{1,0:T(8,128)(2,1)} %wq_ref.1, bf16[16,256]{1,0:T(8,128)(2,1)} %wk_ref.1, bf16[16,256]{1,0:T(8,128)(2,1)} %wv_ref.1, bf16[4,16]{1,0:T(4,128)(2,1)} %bitcast.5, f32[4]{0:T(128)} %off_ref.1, ...), custom_call_target="tpu_custom_call" | custom-call | tf_op jit(solution)/shard_map/pallas_call | solution.py:639
  67.4 1.6 %copy.11 = bf16[64,1024]{1,0:T(8,128)(2,1)} copy(bf16[64,1024]{1,0:T(8,128)(2,1)} %shard_map.91) | data formatting | bytes 262144

commit v6 on v5

--- a/solution.py
+++ b/solution.py
@@ -70,15 +70,15 @@
 
 def kernel(
     dims,
-    tokens_ref,
-    gain_ref,
-    wq_ref,
-    wk_ref,
-    wv_ref,
-    wf_ref,
+    tokens_hbm,
+    gain_hbm,
+    wq_hbm,
+    wk_hbm,
+    wv_hbm,
+    wf_hbm,
     off_ref,
-    wo_ref,
-    ogain_ref,
+    wo_hbm,
+    ogain_hbm,
     out_ref,
     W,
     XN,
@@ -104,14 +104,23 @@
     SC,
     PB,
     WO_OWN,
+    tokens_ref,
+    gain_ref,
+    wq_ref,
+    wk_ref,
+    wv_ref,
+    wf_ref,
+    wo_ref,
+    ogain_ref,
+    in_sems,
     send_sems,
     recv_sems,
 ):
     Z, X, C, Y = dims
-    TB, D = tokens_ref.shape
+    TB, D = tokens_hbm.shape
     GB = TB * Y
     HB = GB // 2
-    PR, WC = wo_ref.shape
+    PR, WC = wo_hbm.shape
     LW = W.shape[2]
     z, x, c, y = (lax.axis_index(a) for a in AXES)
     links = Links(send_sems, recv_sems, K)
@@ -135,6 +144,8 @@
 
     co = 1 - c
     plane = [(dx, dy) for dx in range(X) for dy in range(Y) if (dx, dy) != (0, 0)]
+    plane.sort(key=lambda at: -min(at[0], X - at[0]) - min(at[1], Y - at[1]))
+    x_far = sorted(range(1, X), key=lambda d: -min(d, X - d))
     far_first = sorted(range(1, Z), key=lambda d: -min(d, Z - d))
     near_first = [0] + far_first[::-1]
     x_near, y_near = ([1] if n == 2 else [1, -1] for n in (X, Y))
@@ -145,6 +156,24 @@
     )
     for g in greeted:
         pl.semaphore_signal(barrier, inc=1, device_id=dev(**g), device_id_type=MESH)
+
+    operands = (
+        (wk_hbm, wk_ref),
+        (wv_hbm, wv_ref),
+        (wq_hbm, wq_ref),
+        (wf_hbm, wf_ref),
+        (tokens_hbm, tokens_ref),
+        (gain_hbm, gain_ref),
+        (wo_hbm, wo_ref),
+        (ogain_hbm, ogain_ref),
+    )
+    fetches = [
+        pltpu.make_async_copy(src, dst, in_sems.at[i]) for i, (src, dst) in enumerate(operands)
+    ]
+    for fetch in fetches:
+        fetch.start()
+    for fetch in fetches:
+        fetch.wait()
 
     def w_rows(xx, cc):
         return pl.ds(pl.multiple_of((xx * C + cc) * PR, PR), PR)
@@ -289,7 +318,7 @@
     for h in range(X):
         offset = jnp.where(head_row == h, off_ref[h], offset)
     GS[...] = log_sigmoid(gates + offset + math.log(GB * Z * X * C))
-    for dx in range(1, X):
+    for dx in x_far:
         links.send(("g",), GS, GX.at[x], dev(dx=dx))
     GX[x] = GS[...]
     k_all = project(0, WC)
@@ -357,7 +386,7 @@
     q_all = q_all.T
     for h in range(X):
         QS[h] = q_all[h * HEAD_DIM : (h + 1) * HEAD_DIM].astype(jnp.bfloat16)
-    for dx in range(1, X):
+    for dx in x_far:
         links.send(("q",), QS.at[xrel(dx)], QT.at[x], dev(dx=dx))
     QT[x] = QS[x]
 
@@ -607,6 +636,7 @@
     keys = Z * X * C * HB
     n_sems = 101
     vmem, smem = pl.BlockSpec(memory_space=pltpu.VMEM), pl.BlockSpec(memory_space=pltpu.SMEM)
+    hbm = pl.BlockSpec(memory_space=pltpu.MemorySpace.HBM)
     bf16, f32 = jnp.bfloat16, jnp.float32
     scratch = [
         pltpu.VMEM((Z, X * C * PR, LW), bf16),
@@ -633,13 +663,22 @@
         pltpu.VMEM((3, 2, 2 * HB, GB), f32),
         pltpu.VMEM((2, 4 * HB, GB), bf16),
         pltpu.VMEM((2, PR, WC // 2), bf16),
+        pltpu.VMEM((TB, D), bf16),
+        pltpu.VMEM((1, D), f32),
+        pltpu.VMEM((PR, WC), bf16),
+        pltpu.VMEM((PR, WC), bf16),
+        pltpu.VMEM((PR, WC), bf16),
+        pltpu.VMEM((w_forget.shape[1], PR), bf16),
+        pltpu.VMEM((PR, WC), bf16),
+        pltpu.VMEM((1, D), f32),
+        pltpu.SemaphoreType.DMA((8,)),
         pltpu.SemaphoreType.DMA((5,)),
         pltpu.SemaphoreType.DMA((n_sems,)),
     ]
     return pl.pallas_call(
         functools.partial(kernel, dims),
         out_shape=jax.ShapeDtypeStruct((TB, D), bf16),
-        in_specs=[vmem] * 6 + [smem, vmem, vmem],
+        in_specs=[hbm] * 6 + [smem, hbm, hbm],
         out_specs=vmem,
         scratch_shapes=scratch,
         compiler_params=pltpu.CompilerParams(

time: 69 us -> 68.6 us (level)
  no operation moved by 1% of the time
where the time goes in v6:
time: 68.6 us; the launch traced here: 68.5 us
  Pallas kernels  66.9 us (98%)
  local copies, waits for them, and re-layouts  1.57 us (2%)
    pallas_call x1, Pallas kernels, layer(): pl.pallas_call(functools.partial(kernel, dims), out_shape=jax.ShapeDtypeS...  66.9 us
    unnamed x1, local copies, waits for them, and re-layouts  1.57 us

profile of v6, /device:TPU:224, one launch (start us, length us, event | category | flops | bytes accessed | tf_op | source)
XLA Modules:
  0.0 68.5 jit_solution(8064688152641893943)
XLA Ops:
  0.0 66.9 %shard_map.91 = bf16[64,1024]{1,0:T(8,128)(2,1)} custom-call(bf16[64,1024]{1,0:T(8,128)(2,1)} %tokens_hbm.1, f32[1,1024]{1,0:T(1,128)} %bitcast.3, bf16[16,256]{1,0:T(8,128)(2,1)} %wq_hbm.1, bf16[16,256]{1,0:T(8,128)(2,1)} %wk_hbm.1, bf16[16,256]{1,0:T(8,128)(2,1)} %wv_hbm.1, bf16[4,16]{1,0:T(4,128)(2,1)} %bitcast.5, f32[4]{0:T(128)} %off_ref.1, ...), custom_call_target="tpu_custom_call" | custom-call | tf_op jit(solution)/shard_map/pallas_call | solution.py:678
  66.9 1.6 %copy.11 = bf16[64,1024]{1,0:T(8,128)(2,1)} copy(bf16[64,1024]{1,0:T(8,128)(2,1)} %shard_map.91) | data formatting | bytes 262144

commit v7 on v6

--- a/solution.py
+++ b/solution.py
@@ -274,14 +274,14 @@
         if Y > 2:
             part = t_rows(yrel(-dy), lo, TB // 2)
             links.send(("tok2", dy), part, part, dev(dy=dy))
+    links.recv(("wz", Q), W.at[0 : Z - 1, 0:PR, Q[0] : Q[1]], dev(dz=1))
+    for dx in x_near:
+        view = w_bundle(x, c, Q)
+        links.send(("x1", Q, dx), view, view, dev(dx=dx))
     for d in near_first:
         fine_x(d)
     for dx in x_near:
         to_other_core(xrel(-dx), KVF)
-    links.recv(("wz", Q), W.at[0 : Z - 1, 0:PR, Q[0] : Q[1]], dev(dz=1))
-    for dx in x_near:
-        view = w_bundle(x, c, Q)
-        links.send(("x1", Q, dx), view, view, dev(dx=dx))
     if opposite:
         for d in near_first:
             fine_last(d)

time: 68.6 us -> 67.8 us (0.988)
  Pallas kernels: 66.9 us -> 65.9 us
    pallas_call x1, Pallas kernels: 66.9 us -> 65.9 us  [layer(): pl.pallas_call(functools.partial(kernel, dims), out_shape=jax.ShapeDtypeS...]
where the time goes in v7:
time: 67.8 us; the launch traced here: 67.4 us
  Pallas kernels  65.9 us (97%)
  local copies, waits for them, and re-layouts  1.57 us (2%)
    pallas_call x1, Pallas kernels, layer(): pl.pallas_call(functools.partial(kernel, dims), out_shape=jax.ShapeDtypeS...  65.9 us
    unnamed x1, local copies, waits for them, and re-layouts  1.57 us

profile of v7, /device:TPU:224, one launch (start us, length us, event | category | flops | bytes accessed | tf_op | source)
XLA Modules:
  0.0 67.4 jit_solution(9237151296839602866)
XLA Ops:
  0.0 65.9 %shard_map.91 = bf16[64,1024]{1,0:T(8,128)(2,1)} custom-call(bf16[64,1024]{1,0:T(8,128)(2,1)} %tokens_hbm.1, f32[1,1024]{1,0:T(1,128)} %bitcast.3, bf16[16,256]{1,0:T(8,128)(2,1)} %wq_hbm.1, bf16[16,256]{1,0:T(8,128)(2,1)} %wk_hbm.1, bf16[16,256]{1,0:T(8,128)(2,1)} %wv_hbm.1, bf16[4,16]{1,0:T(4,128)(2,1)} %bitcast.5, f32[4]{0:T(128)} %off_ref.1, ...), custom_call_target="tpu_custom_call" | custom-call | tf_op jit(solution)/shard_map/pallas_call | solution.py:678
  65.9 1.6 %copy.11 = bf16[64,1024]{1,0:T(8,128)(2,1)} copy(bf16[64,1024]{1,0:T(8,128)(2,1)} %shard_map.91) | data formatting | bytes 262144
